TPU v7x, 256 devices: a whole 4x4x8 slice. The times are simulated.
256 devices in a mesh: sp: 64 (over z, y, core), tp: 4 (over x).
Axes of the slice: x: 4, y: 4, z: 8, core: 2. Of those that a mesh axis runs over, the one named last changes fastest.
Arguments:
- layer_grad: bfloat16 [12288, 2048], P('sp'), may hold values from -16 to 16
- routes: int32 [12288, 2], P('sp'), may hold values from 0 to 63, as said below
- route_weight: float32 [12288, 2], P('sp'), may hold values from 0.1 to 0.9
- slot_tokens: bfloat16 [64, 576, 2048], P('sp'), may hold values from -6 to 6
- gate_proj: bfloat16 [64, 2048, 1024], P('sp', None, 'tp'), may hold values from -0.125 to 0.125
- up_proj: bfloat16 [64, 2048, 1024], P('sp', None, 'tp'), may hold values from -0.125 to 0.125
- down_proj: bfloat16 [64, 1024, 2048], P('sp', 'tp'), may hold values from -0.1875 to 0.1875
- out_proj: bfloat16 [2048, 1024], P(None, 'tp'), may hold values from -0.1875 to 0.1875
- queries: bfloat16 [12288, 512], P('sp', 'tp'), may hold values from -6 to 6
- keys: bfloat16 [12288, 512], P('sp', 'tp'), may hold values from -6 to 6
- values: bfloat16 [12288, 1024], P('sp', 'tp'), may hold values from -6 to 6
- fwd_decay: float32 [12288, 512], P('sp', 'tp'), may hold values from -2 to 0
- bwd_decay: float32 [12288, 512], P('sp', 'tp'), may hold values from -2 to 0
Outputs:
- gate_grad: bfloat16 [64, 2048, 1024], P('sp', None, 'tp')
- up_grad: bfloat16 [64, 2048, 1024], P('sp', None, 'tp')
- down_grad: bfloat16 [64, 1024, 2048], P('sp', 'tp')
- proj_grad: float32 [2048, 1024], P('sp', 'tp')
- query_grad: bfloat16 [12288, 512], P('sp', 'tp')
- key_grad: bfloat16 [12288, 512], P('sp', 'tp')
- value_grad: bfloat16 [12288, 1024], P('sp', 'tp')
Inputs may be any that keep to these rules, and one draw needn't show every extreme that they name: `routes`: each row names two different experts of one group of 8 consecutive experts. In every aligned block of 192 rows one expert is named by 9 rows or more.
All inputs are finite; a program needn't handle non-finite values.
Results may differ from a plain program's by a relative error of at most 0.015.
Values may be sent and summed in bfloat16 or wider, within the bound.
A program may use at most 128 MiB of HBM per device.

v0:
```python
import jax
import jax.numpy as jnp
from jax import lax
from jax.sharding import Mesh
from jax.sharding import PartitionSpec as P

KEY_CHANNELS = 64
DV = 128
BLOCK = 64
SP = ("sp_0", "sp_1", "sp_2")


EPSILON = 1e-06


def filled_with(array, identity):
    return jax.tree.map(
        lambda a, e: jnp.broadcast_to(jnp.asarray(e, a.dtype), a.shape), array, identity
    )


def all_in_one(array, axis):
    leaves = jax.tree.leaves(array)
    sequence = sorted(range(len(leaves)), key=lambda k: -leaves[k].size)
    width = (1, *leaves[sequence[0]].shape)[-1]
    lines = [
        jnp.pad(leaves[k].reshape(-1), (0, -leaves[k].size % width)).reshape(-1, width)
        for k in sequence
    ]
    both, at, found = (lax.all_gather(jnp.concatenate(lines), axis), 0, {})
    for k, line in zip(sequence, lines):
        slab = both[:, at : at + len(line)].reshape(len(both), -1)
        found[k] = slab[:, : leaves[k].size].reshape(-1, *leaves[k].shape)
        at += len(line)
    numbers = iter(range(len(leaves)))
    return jax.tree.map(lambda _: found[next(numbers)], array)


def once_a_type(array, axis):
    leaves, found = (jax.tree.leaves(array), {})
    for leading, a in enumerate(leaves):
        if leading not in found:
            alike = [k for k, b in enumerate(leaves) if b.dtype == a.dtype]
            got = (
                all_in_one([leaves[k] for k in alike], axis)
                if len(alike) > 1
                else [lax.all_gather(a, axis)]
            )
            for k, b in zip(alike, got):
                found[k] = b
    numbers = iter(range(len(leaves)))
    return jax.tree.map(lambda _: found[next(numbers)], array)


def carried_in(array, axes, combine, identity, reverse):
    before = start = filled_with(array, identity)
    total = array
    for axis in reversed(axes):
        devices, index = (lax.axis_size(axis), lax.axis_index(axis))
        pieces = once_a_type(total, axis)
        inside, total = (start, start)
        for k in reversed(range(devices)) if reverse else range(devices):
            passed = k > index if reverse else k < index
            total = combine(total, jax.tree.map(lambda part: part[k], pieces))
            inside = jax.tree.map(lambda new, old: jnp.where(passed, new, old), total, inside)
        before = combine(inside, before)
    return before


def copy_for_each(array, axis):
    devices = lax.axis_size(axis)
    return lax.all_to_all(
        jnp.broadcast_to(array[None], (devices, *array.shape)), axis, 0, 0, tiled=True
    )


def in_order(pieces, dim):
    shape = list(pieces.shape[1:])
    shape[dim] *= pieces.shape[0]
    return jnp.moveaxis(pieces, 0, dim).reshape(shape)


def gathered_copies(array, axis, dim):
    pieces = copy_for_each(array, axis)
    return in_order(pieces, dim)


def split_up(array, dim, devices):
    before, after = (array.shape[:dim], array.shape[dim + 1 :])
    return jnp.moveaxis(array.reshape(*before, devices, -1, *after), dim, 0)


def sum_at_owner(array, axis, dim):
    pieces = split_up(array, dim, lax.axis_size(axis))
    arrived = lax.all_to_all(pieces, axis, split_axis=0, concat_axis=0, tiled=True)
    return arrived.sum(axis=0)


def sweep(query_rows, keyrows, valrows, log_decay, strict):
    nheads, length, kwidth = query_rows.shape
    vwidth = valrows.shape[-1]
    number = length // BLOCK
    offset = -1 if strict else 0
    causal = jnp.tril(jnp.ones((BLOCK, BLOCK), jnp.float32), offset)

    def split(array):
        return jnp.moveaxis(array.reshape(nheads, number, BLOCK, array.shape[-1]), 1, 0)

    def advance(carried_state, pieces):
        query_block, key_block, value_block, gblock = pieces
        running_total = jnp.cumsum(gblock, axis=1)
        middle = running_total[:, BLOCK // 2 - 1 : BLOCK // 2, :]
        scores = (
            jnp.einsum(
                "hik,hjk->hij",
                query_block * jnp.exp(running_total - middle),
                key_block * jnp.exp(middle - running_total),
            )
            * causal
        )
        inner = jnp.einsum("hij,hjv->hiv", scores, value_block)
        outer_product = jnp.einsum(
            "zuw,zwo->zuo", query_block * jnp.exp(running_total), carried_state
        )
        final_row = running_total[:, -1:, :]
        fresh_state = jnp.einsum(
            "xor,xot->xrt", key_block * jnp.exp(final_row - running_total), value_block
        )
        return (
            jnp.exp(final_row[:, 0, :])[:, :, None] * carried_state + fresh_state,
            inner + outer_product,
        )

    start_state = jnp.zeros((nheads, kwidth, vwidth), jnp.float32)
    final, outputs = lax.scan(
        advance, start_state, (split(query_rows), split(keyrows), split(valrows), split(log_decay))
    )
    return (jnp.moveaxis(outputs, 0, 1).reshape(nheads, length, vwidth), final)


def slot_ranks(expert_ids, experts):
    members = (expert_ids[:, None] == jnp.arange(experts, dtype=jnp.int32)[None, :]).astype(
        jnp.int32
    )
    before = jnp.cumsum(members, axis=0) - members
    return jnp.sum(before * members, axis=1)


def local_pass(query_rows, keyrows, valrows, fwd_log, bwd_log):
    forward_out, forward_end = sweep(query_rows, keyrows, valrows, fwd_log, False)
    backward_out, backward_end = sweep(
        jnp.flip(query_rows, 1),
        jnp.flip(keyrows, 1),
        jnp.flip(valrows, 1),
        jnp.flip(bwd_log, 1),
        True,
    )
    return (forward_out, forward_end, jnp.flip(backward_out, 1), backward_end)


def finish(query_rows, fwd_log, bwd_log, forward_out, backward_out, forward_entry, backward_entry):
    rising_decay = jnp.exp(jnp.cumsum(fwd_log, axis=1))
    falling_decay = jnp.exp(jnp.flip(jnp.cumsum(jnp.flip(bwd_log, 1), axis=1), 1))
    mixed = forward_out + backward_out
    mixed = mixed + jnp.einsum("xfj,xji->xfi", query_rows * rising_decay, forward_entry)
    mixed = mixed + jnp.einsum("xfj,xji->xfi", query_rows * falling_decay, backward_entry)
    return mixed * lax.rsqrt(jnp.mean(mixed * mixed, axis=-1, keepdims=True) + EPSILON)


def combine(earlier, later):
    return (earlier[0] * later[0], later[0][:, :, None] * earlier[1] + later[1])


def carry(decays, terms, backward):
    identity = (jnp.ones_like(decays), jnp.zeros_like(terms))
    return carried_in((decays, terms), SP, combine, identity, backward)[1]


def on_device(
    layer_grad,
    routes,
    route_weight,
    slot_tokens,
    gate_proj,
    up_proj,
    down_proj,
    out_proj,
    queries,
    keys,
    values,
    fwd_decay,
    bwd_decay,
):
    devices = lax.axis_size(SP)
    rows_here = layer_grad.shape[0]
    width = layer_grad.shape[1]
    slots = slot_tokens.shape[1]
    capacity = slots // devices
    expert_ids = routes.reshape(-1)
    ranks = slot_ranks(expert_ids, devices)
    kept = ranks < capacity
    target = jnp.where(kept, expert_ids * capacity + ranks, slots)
    sender = (
        jnp.full((slots + 1,), -1, jnp.int32)
        .at[target]
        .set(jnp.arange(2 * rows_here, dtype=jnp.int32))[:slots]
    )
    anchor = jnp.maximum(sender, 0)
    scaled = route_weight.reshape(-1)[anchor] * (sender >= 0).astype(jnp.float32)
    column_share = width // lax.axis_size("tp")
    own_slice = lax.dynamic_slice_in_dim(
        layer_grad, lax.axis_index("tp") * column_share, column_share, 1
    )
    outgoing = (own_slice[anchor // 2].astype(jnp.float32) * scaled[:, None]).astype(jnp.bfloat16)
    arrived = lax.all_to_all(
        outgoing.reshape(devices, capacity, column_share),
        SP,
        split_axis=0,
        concat_axis=0,
        tiled=True,
    ).reshape(slots, column_share)
    inbound = gathered_copies(arrived, "tp", 1)
    inputs = slot_tokens[0]
    w_gate = gate_proj[0]
    w_upper = up_proj[0]
    w_down = down_proj[0]
    gate = jnp.dot(inputs, w_gate, preferred_element_type=jnp.float32)
    upper = jnp.dot(inputs, w_upper, preferred_element_type=jnp.float32)
    sigma = jax.nn.sigmoid(gate)
    act = (gate * sigma * upper).astype(jnp.bfloat16)
    grad_down = lax.dot_general(
        act, inbound, (((0,), (0,)), ((), ())), preferred_element_type=jnp.float32
    )
    act_grad = lax.dot_general(
        inbound, w_down, (((1,), (1,)), ((), ())), preferred_element_type=jnp.float32
    )
    up_delta = (act_grad * gate * sigma).astype(jnp.bfloat16)
    gate_delta = (act_grad * upper * sigma * (1.0 + gate * (1.0 - sigma))).astype(jnp.bfloat16)
    grad_gate = lax.dot_general(
        inputs, gate_delta, (((0,), (0,)), ((), ())), preferred_element_type=jnp.float32
    )
    grad_up = lax.dot_general(
        inputs, up_delta, (((0,), (0,)), ((), ())), preferred_element_type=jnp.float32
    )
    slot_part = lax.dot_general(
        gate_delta, w_gate, (((1,), (1,)), ((), ())), preferred_element_type=jnp.float32
    )
    slot_part = slot_part + lax.dot_general(
        up_delta, w_upper, (((1,), (1,)), ((), ())), preferred_element_type=jnp.float32
    )
    safe_target = jnp.minimum(target, slots - 1)
    kept_float = kept.astype(jnp.float32)[:, None]
    quarter = width // lax.axis_size("tp")
    summed = lax.psum_scatter(slot_part.astype(jnp.bfloat16), "tp", scatter_dimension=1, tiled=True)
    backrows = lax.all_to_all(
        summed.reshape(devices, capacity, quarter), SP, split_axis=0, concat_axis=0, tiled=True
    ).reshape(slots, quarter)
    picked = backrows[safe_target].astype(jnp.float32) * kept_float
    moe_grad = jnp.sum(picked.reshape(rows_here, 2, quarter), axis=1)
    own_columns = lax.dynamic_slice_in_dim(layer_grad, lax.axis_index("tp") * quarter, quarter, 1)
    stream_part = (own_columns.astype(jnp.float32) + moe_grad).astype(jnp.bfloat16)
    stream_grad = lax.all_gather(stream_part, "tp", axis=1, tiled=True)
    scale = KEY_CHANNELS ** (-0.5)

    def split_heads(array, size):
        return array.astype(jnp.float32).reshape(rows_here, -1, size).transpose(1, 0, 2)

    def merge_heads(array):
        return array.transpose(1, 0, 2).reshape(rows_here, -1)

    query_heads = split_heads(queries, KEY_CHANNELS) * scale
    fwd_heads = split_heads(fwd_decay, KEY_CHANNELS)
    bwd_heads = split_heads(bwd_decay, KEY_CHANNELS)
    local_out, local_pull = jax.vjp(
        local_pass,
        query_heads,
        split_heads(keys, KEY_CHANNELS),
        split_heads(values, DV),
        fwd_heads,
        bwd_heads,
    )
    forward_out, forward_end, backward_out, backward_end = local_out
    fwd_total = jnp.exp(jnp.sum(fwd_heads, axis=1))
    bwd_total = jnp.exp(jnp.sum(bwd_heads, axis=1))
    forward_entry = carry(fwd_total, forward_end, False)
    backward_entry = carry(bwd_total, backward_end, True)
    mixed, finish_pull = jax.vjp(
        finish,
        query_heads,
        fwd_heads,
        bwd_heads,
        forward_out,
        backward_out,
        forward_entry,
        backward_entry,
    )
    mixed_rows = merge_heads(mixed).astype(jnp.bfloat16)
    proj_grad = sum_at_owner(
        lax.dot_general(
            stream_grad, mixed_rows, (((0,), (0,)), ((), ())), preferred_element_type=jnp.float32
        ),
        SP,
        0,
    )
    mixed_grad = jnp.dot(stream_grad, out_proj, preferred_element_type=jnp.float32)
    query_first, fwd_first, bwd_first, forward_cot, backward_cot, fwd_direct, bwd_direct = (
        finish_pull(split_heads(mixed_grad, DV))
    )
    fwd_after = carry(fwd_total, fwd_direct, True)
    bwd_after = carry(bwd_total, bwd_direct, False)
    query_second, key_part, value_part, fwd_unused, bwd_unused = local_pull(
        (forward_cot, fwd_after, backward_cot, bwd_after)
    )
    query_grad = (merge_heads(query_first + query_second) * scale).astype(jnp.bfloat16)
    return (
        grad_gate.astype(jnp.bfloat16)[None],
        grad_up.astype(jnp.bfloat16)[None],
        grad_down.astype(jnp.bfloat16)[None],
        proj_grad,
        query_grad,
        merge_heads(key_part).astype(jnp.bfloat16),
        merge_heads(value_part).astype(jnp.bfloat16),
    )


def solution(mesh):
    torus = Mesh(mesh.devices.reshape(8, 4, 2, mesh.shape["tp"]), ("sp_0", "sp_1", "sp_2", "tp"))
    in_specs = (
        P(SP, None),
        P(SP, None),
        P(SP, None),
        P(SP, None, None),
        P(SP, None, "tp"),
        P(SP, None, "tp"),
        P(SP, "tp", None),
        P(None, "tp"),
        P(SP, "tp"),
        P(SP, "tp"),
        P(SP, "tp"),
        P(SP, "tp"),
        P(SP, "tp"),
    )
    out_specs = (
        P(SP, None, "tp"),
        P(SP, None, "tp"),
        P(SP, "tp", None),
        P(SP, "tp"),
        P(SP, "tp"),
        P(SP, "tp"),
        P(SP, "tp"),
    )
    return jax.shard_map(
        on_device, mesh=torus, in_specs=in_specs, out_specs=out_specs, check_vma=False
    )
```

profile of v0, /device:TPU:1, one launch (start us, length us, event | category | flops | bytes accessed | tf_op | source)
XLA Modules:
  0.0 496.6 jit_solution(14228876233473937465)
XLA Ops:
  19.8 4.0 gather_fusion.1
  26.7 13.5 %all-to-all-start = ((bf16[64,9,512]{2,1,0:T(8,128)(2,1)}), bf16[64,9,512]{2,1,0:T(8,128)(2,1)}, u32[]{:S(2)}, u32[]{:S(2)}) async-start(bf16[64,9,512]{2,1,0:T(8,128)(2,1)} %multiply_convert_fusion), calls=%async_computation | async-start | bytes 2097152 | tf_op jit(solution)/shard_map/all_to_all | solution.py:215
  57.9 17.1 %while.115 = (s32[]{:T(128)}, f32[2,64,128]{2,1,0:T(8,128)S(1)}, f32[3,2,64,128]{3,2,1,0:T(8,128)}, f32[3,2,64,64]{3,2,1,0:T(8,128)}, f32[3,2,64,64]{3,2,1,0:T(8...) while((s32[]{:T(128)}, f32[2,64,128]{2,1,0:T(8,128)S(1)}, ...), condition=%wide.region_11.12_spmd.clone, body=%wide.region_9.11_spmd.clone.sunk | while | flops 8093699 | bytes 2081263 | solution.py:135
  82.1 12.8 %while.114 = (s32[]{:T(128)}, f32[2,64,128]{2,1,0:T(8,128)S(1)}, f32[3,2,64,128]{3,2,1,0:T(8,128)}, f32[3,2,64,64]{3,2,1,0:T(8,128)}, f32[3,2,64,64]{3,2,1,0:T(8...) while((s32[]{:T(128)}, f32[2,64,128]{2,1,0:T(8,128)S(1)}, ...), condition=%wide.region_8.9_spmd.clone, body=%wide.region_6.8_spmd.clone.sunk | while | flops 8093699 | bytes 1981671 | solution.py:135
  103.1 10.3 %all-gather.13 = f32[4,129,128]{2,1,0:T(8,128)S(1)} all-gather(f32[1,129,128]{2,1,0:T(8,128)S(1)} %maximum_bitcast_fusion), channel_id=3, replica_groups=mesh['sp_0'=8,'sp_1'=4,'sp_2'=2,'tp'=4] {'sp_1'}, dimensions={0}, use_global_device_ids=true | all-gather | bytes 330240 | tf_op jit(solution)/shard_map/all_gather | solution.py:30
  118.3 4.6 all-to-all-start.1
  123.0 4.2 all-gather.15
  127.9 10.8 %all-gather.16 = f32[4,129,128]{2,1,0:T(8,128)S(1)} all-gather(f32[1,129,128]{2,1,0:T(8,128)S(1)} %maximum_bitcast_fusion.2), channel_id=6, replica_groups=mesh['sp_0'=8,'sp_1'=4,'sp_2'=2,'tp'=4] {'sp_1'}, dimensions={0}, use_global_device_ids=true | all-gather | bytes 330240 | tf_op jit(solution)/shard_map/all_gather | solution.py:30
  144.0 5.6 %all-to-all-done.1 = bf16[4,576,512]{2,1,0:T(8,128)(2,1)} async-done(((bf16[4,576,512]{2,1,0:T(8,128)(2,1)}), bf16[4,576,512]{2,1,0:T(8,128)(2,1)}, u32[]{:S(2)}, u32[]{:S(2)}) %all-to-all-start.1) | async-done | bytes 2359328 | tf_op jit(solution)/shard_map/all_to_all | solution.py:72
  157.4 21.8 %all-gather.14 = f32[8,129,128]{2,1,0:T(8,128)S(1)} all-gather(f32[1,129,128]{2,1,0:T(8,128)S(1)} %maximum_bitcast_fusion.1), channel_id=4, replica_groups=mesh['sp_0'=8,'sp_1'=4,'sp_2'=2,'tp'=4] {'sp_0'}, dimensions={0}, use_global_device_ids=true | all-gather | bytes 594432 | tf_op jit(solution)/shard_map/all_gather | solution.py:30
  179.2 20.9 %all-gather.17 = f32[8,129,128]{2,1,0:T(8,128)S(1)} all-gather(f32[1,129,128]{2,1,0:T(8,128)S(1)} %maximum_bitcast_fusion.3), channel_id=7, replica_groups=mesh['sp_0'=8,'sp_1'=4,'sp_2'=2,'tp'=4] {'sp_0'}, dimensions={0}, use_global_device_ids=true | all-gather | bytes 594432 | tf_op jit(solution)/shard_map/all_gather | solution.py:30
  234.4 20.6 %all-to-all-start.2 = ((bf16[64,9,512]{2,1,0:T(8,128)(2,1)}), bf16[64,9,512]{2,1,0:T(8,128)(2,1)}, u32[]{:S(2)}, u32[]{:S(2)}) async-start(bf16[64,9,512]{2,1,0:T(8,128)(2,1)} %reshape.1346), calls=%async_computation.3 | async-start | bytes 2097152 | tf_op jit(solution)/shard_map/all_to_all | solution.py:255
  265.0 4.0 fusion.172
  269.0 14.0 %all-to-all-done.2 = bf16[64,9,512]{2,1,0:T(8,128)(2,1)} async-done(((bf16[64,9,512]{2,1,0:T(8,128)(2,1)}), bf16[64,9,512]{2,1,0:T(8,128)(2,1)}, u32[]{:S(2)}, u32[]{:S(2)}) %all-to-all-start.2) | async-done | bytes 589856 | tf_op jit(solution)/shard_map/all_to_all | solution.py:255
  291.6 11.2 %all_gather.75 = bf16[192,2048]{1,0:T(8,128)(2,1)S(1)} all-gather(bf16[192,512]{1,0:T(8,128)(2,1)S(1)} %add_convert_fusion.1), channel_id=1, replica_groups=mesh['sp_0'=8,'sp_1'=4,'sp_2'=2,'tp'=4] {'tp'}, dimensions={1}, use_global_device_ids=true | all-gather | bytes 983040 | tf_op jit(solution)/shard_map/all_gather | solution.py:262
  305.0 5.7 %all-gather.21 = f32[2,129,128]{2,1,0:T(8,128)S(1)} all-gather(f32[1,129,128]{2,1,0:T(8,128)S(1)} %fusion.205), channel_id=11, replica_groups=mesh['sp_0'=8,'sp_1'=4,'sp_2'=2,'tp'=4] {'sp_2'}, dimensions={0}, use_global_device_ids=true | all-gather | bytes 198144 | tf_op jit(solution)/shard_map/all_gather | solution.py:30
  312.1 10.1 %all-gather.22 = f32[4,129,128]{2,1,0:T(8,128)S(1)} all-gather(f32[1,129,128]{2,1,0:T(8,128)S(1)} %maximum_bitcast_fusion.6), channel_id=12, replica_groups=mesh['sp_0'=8,'sp_1'=4,'sp_2'=2,'tp'=4] {'sp_1'}, dimensions={0}, use_global_device_ids=true | all-gather | bytes 330240 | tf_op jit(solution)/shard_map/all_gather | solution.py:30
  323.6 19.7 %all-gather.23 = f32[8,129,128]{2,1,0:T(8,128)S(1)} all-gather(f32[1,129,128]{2,1,0:T(8,128)S(1)} %maximum_bitcast_fusion.7), channel_id=13, replica_groups=mesh['sp_0'=8,'sp_1'=4,'sp_2'=2,'tp'=4] {'sp_0'}, dimensions={0}, use_global_device_ids=true | all-gather | bytes 594432 | tf_op jit(solution)/shard_map/all_gather | solution.py:30
  345.0 10.6 %all-gather.18 = f32[2,129,128]{2,1,0:T(8,128)S(1)} all-gather(f32[1,129,128]{2,1,0:T(8,128)S(1)} %fusion.203), channel_id=8, replica_groups=mesh['sp_0'=8,'sp_1'=4,'sp_2'=2,'tp'=4] {'sp_2'}, dimensions={0}, use_global_device_ids=true | all-gather | bytes 198144 | tf_op jit(solution)/shard_map/all_gather | solution.py:30
  356.9 10.0 %all-gather.19 = f32[4,129,128]{2,1,0:T(8,128)S(1)} all-gather(f32[1,129,128]{2,1,0:T(8,128)S(1)} %maximum_bitcast_fusion.4), channel_id=9, replica_groups=mesh['sp_0'=8,'sp_1'=4,'sp_2'=2,'tp'=4] {'sp_1'}, dimensions={0}, use_global_device_ids=true | all-gather | bytes 330240 | tf_op jit(solution)/shard_map/all_gather | solution.py:30
  368.4 20.1 %all-gather.20 = f32[8,129,128]{2,1,0:T(8,128)S(1)} all-gather(f32[1,129,128]{2,1,0:T(8,128)S(1)} %maximum_bitcast_fusion.5), channel_id=10, replica_groups=mesh['sp_0'=8,'sp_1'=4,'sp_2'=2,'tp'=4] {'sp_0'}, dimensions={0}, use_global_device_ids=true | all-gather | bytes 594432 | tf_op jit(solution)/shard_map/all_gather | solution.py:30
  396.1 13.9 %all-to-all-start.3 = ((f32[64,32,256]{2,1,0:T(8,128)}), f32[64,32,256]{2,1,0:T(8,128)}, u32[]{:S(2)}, u32[]{:S(2)}) async-start(f32[64,32,256]{2,1,0:T(8,128)} %fusion.253), calls=%async_computation.4 | async-start | bytes 4194304 | tf_op jit(solution)/shard_map/all_to_all | solution.py:95
  422.0 23.2 %while.112 = (s32[]{:T(128)}, f32[2,64,128]{2,1,0:T(8,128)S(1)}, f32[3,2,64,64]{3,2,1,0:T(8,128)S(1)}, f32[3,2,64,64]{3,2,1,0:T(8,128)S(1)}, f32[3,2,64,128]{3,2...) while((s32[]{:T(128)}, f32[2,64,128]{2,1,0:T(8,128)S(1)}, ...), condition=%wide.region_22.23_spmd.clone, body=%wide.region_21.22_spmd.clone.sunk | while | flops 14802947 | bytes 1518041 | solution.py:135
  449.0 24.9 %while.113 = (s32[]{:T(128)}, f32[2,64,128]{2,1,0:T(8,128)S(1)}, f32[3,2,64,64]{3,2,1,0:T(8,128)S(1)}, f32[3,2,64,64]{3,2,1,0:T(8,128)}, f32[3,2,64,128]{3,2,0,1...) while((s32[]{:T(128)}, f32[2,64,128]{2,1,0:T(8,128)S(1)}, ...), condition=%wide.region_24.25_spmd.clone, body=%wide.region_23.24_spmd.clone.sunk | while | flops 14802947 | bytes 1501393 | solution.py:135
  (648 shorter events, 244.7 us)
Async XLA Ops:
  7.2 132.2 %copy-start = (bf16[1,576,2048]{2,1,0:T(8,128)(2,1)S(1)}, bf16[1,576,2048]{2,1,0:T(8,128)(2,1)}, u32[]{:S(2)}) copy-start(bf16[1,576,2048]{2,1,0:T(8,128)(2,1)} %param.24) | copy-start | bytes 7077892
  26.7 88.6 %all-to-all-start = ((bf16[64,9,512]{2,1,0:T(8,128)(2,1)}), bf16[64,9,512]{2,1,0:T(8,128)(2,1)}, u32[]{:S(2)}, u32[]{:S(2)}) async-start(bf16[64,9,512]{2,1,0:T(8,128)(2,1)} %multiply_convert_fusion), calls=%async_computation | async-start | bytes 2097152 | tf_op jit(solution)/shard_map/all_to_all | solution.py:215
  114.1 109.7 %copy-start.62 = (f32[2,64]{1,0:T(2,128)}, f32[2,64]{1,0:T(2,128)S(1)}, u32[]{:S(2)}) copy-start(f32[2,64]{1,0:T(2,128)S(1)} %squeeze.560) | copy-start | bytes 1540
  114.2 109.7 %copy-start.64 = (f32[2,64]{1,0:T(2,128)}, f32[2,64]{1,0:T(2,128)S(1)}, u32[]{:S(2)}) copy-start(f32[2,64]{1,0:T(2,128)S(1)} %squeeze.559) | copy-start | bytes 1540
  114.3 109.6 %copy-start.66 = (f32[2,64]{1,0:T(2,128)}, f32[2,64]{1,0:T(2,128)S(1)}, u32[]{:S(2)}) copy-start(f32[2,64]{1,0:T(2,128)S(1)} %squeeze.558) | copy-start | bytes 1540
  115.0 108.9 %copy-start.68 = (f32[2,64]{1,0:T(2,128)}, f32[2,64]{1,0:T(2,128)S(1)}, u32[]{:S(2)}) copy-start(f32[2,64]{1,0:T(2,128)S(1)} %squeeze.562) | copy-start | bytes 1540
  118.3 31.3 %all-to-all-start.1 = ((bf16[4,576,512]{2,1,0:T(8,128)(2,1)}), bf16[4,576,512]{2,1,0:T(8,128)(2,1)}, u32[]{:S(2)}, u32[]{:S(2)}) async-start(bf16[4,576,512]{2,1,0:T(8,128)(2,1)} %broadcast_in_dim.154), calls=%async_computation.1 | async-start | bytes 4718592 | tf_op jit(solution)/shard_map/all_to_all | solution.py:72
  122.9 109.2 %reduce-scatter.2.cloned.1.call-start = ((), (), s32[]{:S(2)}) async-start(), calls=%async_computation.5 | async-start | bytes 2949120 | tf_op jit(solution)/shard_map/reduce_scatter | solution.py:254
  157.2 46.5 %copy-start.16 = (f32[192,128]{0,1:T(8,128)S(1)}, f32[192,128]{0,1:T(8,128)}, u32[]{:S(2)}) copy-start(f32[192,128]{0,1:T(8,128)} %copy-done.15) | copy-start | bytes 294916
  157.2 51.9 %copy-start.116 = (f32[128]{0:T(128)S(1)}, f32[128]{0:T(128)}, u32[]{:S(2)}) copy-start(f32[128]{0:T(128)} %get-tuple-element.1529) | copy-start | bytes 1540
  157.2 66.6 %copy-start.61 = (s32[384]{0:T(512)S(1)}, s32[384]{0:T(512)}, u32[]{:S(2)}) copy-start(s32[384]{0:T(512)} %get-tuple-element.1545) | copy-start | bytes 4612
  157.2 66.7 %copy-start.91 = (f32[2,64]{1,0:T(2,128)S(1)}, f32[2,64]{1,0:T(2,128)}, u32[]{:S(2)}) copy-start(f32[2,64]{1,0:T(2,128)} %squeeze.557) | copy-start | bytes 1540
  157.2 66.7 %copy-start.92 = (f32[2,64]{1,0:T(2,128)S(1)}, f32[2,64]{1,0:T(2,128)}, u32[]{:S(2)}) copy-start(f32[2,64]{1,0:T(2,128)} %squeeze.561) | copy-start | bytes 1540
  234.4 48.6 %all-to-all-start.2 = ((bf16[64,9,512]{2,1,0:T(8,128)(2,1)}), bf16[64,9,512]{2,1,0:T(8,128)(2,1)}, u32[]{:S(2)}, u32[]{:S(2)}) async-start(bf16[64,9,512]{2,1,0:T(8,128)(2,1)} %reshape.1346), calls=%async_computation.3 | async-start | bytes 2097152 | tf_op jit(solution)/shard_map/all_to_all | solution.py:255
  256.5 46.7 %copy-start.45 = (bf16[2,64,128]{2,1,0:T(8,128)(2,1)}, bf16[2,64,128]{2,1,0:T(8,128)(2,1)S(1)}, u32[]{:S(2)}) copy-start(bf16[2,64,128]{2,1,0:T(8,128)(2,1)S(1)} %add_add_fusion.3) | copy-start | bytes 98308
  304.8 40.2 %copy-start.4 = (bf16[2,192,128]{2,1,0:T(8,128)(2,1)}, bf16[2,192,128]{2,1,0:T(8,128)(2,1)S(1)}, u32[]{:S(2)}) copy-start(bf16[2,192,128]{2,1,0:T(8,128)(2,1)S(1)} %add_add_fusion) | copy-start | bytes 294916
  304.8 40.2 %copy-start.83 = (f32[1,128]{1,0:T(1,128)S(1)}, f32[1,128]{1,0:T(1,128)}, u32[]{:S(2)}) copy-start(f32[1,128]{1,0:T(1,128)} %copy-done.82) | copy-start | bytes 1540
  345.0 44.9 %copy-start.5 = (bf16[2,192,128]{2,1,0:T(8,128)(2,1)S(1)}, bf16[2,192,128]{2,1,0:T(8,128)(2,1)}, u32[]{:S(2)}) copy-start(bf16[2,192,128]{2,1,0:T(8,128)(2,1)} %copy-done.4) | copy-start | bytes 294916
  366.9 25.7 %copy-start.44 = (bf16[192,2,128]{2,0,1:T(8,128)(2,1)S(1)}, bf16[192,2,128]{2,0,1:T(8,128)(2,1)}, u32[]{:S(2)}) copy-start(bf16[192,2,128]{2,0,1:T(8,128)(2,1)} %fusion.197) | copy-start | bytes 294916
  396.1 91.3 %all-to-all-start.3 = ((f32[64,32,256]{2,1,0:T(8,128)}), f32[64,32,256]{2,1,0:T(8,128)}, u32[]{:S(2)}, u32[]{:S(2)}) async-start(f32[64,32,256]{2,1,0:T(8,128)} %fusion.253), calls=%async_computation.4 | async-start | bytes 4194304 | tf_op jit(solution)/shard_map/all_to_all | solution.py:95
  422.0 27.0 %copy-start.3 = (bf16[3,2,64,128]{3,2,1,0:T(8,128)(2,1)S(1)}, bf16[3,2,64,128]{3,2,1,0:T(8,128)(2,1)}, u32[]{:S(2)}) copy-start(bf16[3,2,64,128]{3,2,1,0:T(8,128)(2,1)} %copy-done.2) | copy-start | bytes 294916
  448.9 33.0 %copy-start.14 = (f32[2,256,64]{1,2,0:T(8,128)S(1)}, f32[2,256,64]{1,2,0:T(8,128)}, u32[]{:S(2)}) copy-start(f32[2,256,64]{1,2,0:T(8,128)} %reverse.7) | copy-start | bytes 393220
  449.0 33.0 %copy-start.46 = (bf16[2,64,128]{2,1,0:T(8,128)(2,1)S(1)}, bf16[2,64,128]{2,1,0:T(8,128)(2,1)}, u32[]{:S(2)}) copy-start(bf16[2,64,128]{2,1,0:T(8,128)(2,1)} %copy-done.45) | copy-start | bytes 98308
  449.0 33.2 %copy-start.19 = (f32[2,256,64]{1,2,0:T(8,128)S(1)}, f32[2,256,64]{1,2,0:T(8,128)}, u32[]{:S(2)}) copy-start(f32[2,256,64]{1,2,0:T(8,128)} %copy-done.17) | copy-start | bytes 393220
  (103 other events, 1502.4 us)
Sparse Core Ops, SparseCore 0:
  157.3 35.1 reduce-scatter.1
where the time goes:
time: 502 us; the launch traced here: 497 us
  blocking collectives  157 us (31%)
  local copies, waits for them, and re-layouts  119 us (24%)
  matrix products  84.1 us (17%)
  starting transfers between devices  52.6 us (10%)
  other arithmetic  47.3 us (9%)
  waiting for transfers between devices  19.6 us (4%)
  between operations  16 us (3%)
    all_gather x12, blocking collectives, all_in_one(): both, at, found = (lax.all_gather(jnp.concatenate(lines), axis), 0, {})  146 us
    unnamed x272, local copies, waits for them, and re-layouts  24 us
    dot_general x18, matrix products, advance(): jnp.einsum('hik,hjk->hij', query_block * jnp.exp(running_total - middle),...  21 us
    all_to_all x1, starting transfers between devices, on_device(): lax.all_to_all(summed.reshape(devices, capacity, quarter), SP, split_axis...  20.6 us
    dot_general x18, matrix products, advance(): jnp.einsum('zuw,zwo->zuo', query_block * jnp.exp(running_total), carried_...  16.4 us
    mul x32, local copies, waits for them, and re-layouts, combine(): return (earlier[0] * later[0], later[0][:, :, None] * earlier[1] + later[1])  15.3 us
    all_to_all x1, waiting for transfers between devices, on_device(): lax.all_to_all(summed.reshape(devices, capacity, quarter), SP, split_axis...  14 us
    all_to_all x1, starting transfers between devices, sum_at_owner(): lax.all_to_all(pieces, axis, split_axis=0, concat_axis=0, tiled=True)  13.9 us
  transfers between devices with their start and end apart: 5, of which 2 were waited for; matrix products, arithmetic and copies ran while one was open for 38% of the time, Pallas kernels for 0%

commit v1 on v0

v1 whole, which is shorter than its diff:
```python
import functools

import jax
import jax.numpy as jnp
from jax import lax
from jax.experimental import pallas as pl
from jax.experimental.pallas import tpu as pltpu
from jax.sharding import Mesh
from jax.sharding import PartitionSpec as P

KEY_CHANNELS = 64
DV = 128
BLOCK = 64
SP = ("sp_0", "sp_1", "sp_2")
EPSILON = 1e-06
CAP = 9
F32 = jnp.float32
BF16 = jnp.bfloat16
PIECE = 16
ROWS = PIECE + 8


def dot(a, b, contract=((1,), (0,))):
    return lax.dot_general(
        a.astype(BF16), b.astype(BF16), (contract, ((), ())), preferred_element_type=F32
    )


def dot_exact(a, b):
    return lax.dot_general(
        a,
        b,
        (((1,), (0,)), ((), ())),
        precision=lax.Precision.HIGHEST,
        preferred_element_type=F32,
    )


NT = ((1,), (1,))
TN = ((0,), (0,))


def iota(shape, dim):
    return lax.broadcasted_iota(jnp.int32, shape, dim)


def stacked(x):
    low = iota(x.shape, 1) < KEY_CHANNELS
    zero = jnp.zeros_like(x)
    return jnp.concatenate([jnp.where(low, x, zero), jnp.where(low, zero, x)], axis=0)


def doubled(x):
    return jnp.concatenate([x, x], axis=0)


def folded(x):
    half = x.shape[0] // 2
    return x[:half] + x[half:]


def heads_on_rows(x):
    return jnp.concatenate([x[:, :DV], x[:, DV:]], axis=0)


def heads_on_lanes(x):
    half = x.shape[0] // 2
    return jnp.concatenate([x[:half], x[half:]], axis=1)


def masks():
    shape = (2 * BLOCK, 2 * BLOCK)
    i, j = iota(shape, 0), iota(shape, 1)
    same = (i // BLOCK) == (j // BLOCK)
    return same & (i >= j), same & (i < j)


class Piece:
    def __init__(self, b, q_ref, k_ref, v_ref, fd_ref, bd_ref):
        rows = pl.ds(b * BLOCK, BLOCK)
        shape = (BLOCK, BLOCK)
        lower = (iota(shape, 0) >= iota(shape, 1)).astype(F32)
        upper = (iota(shape, 0) <= iota(shape, 1)).astype(F32)
        self.q = q_ref[rows, :].astype(F32) * KEY_CHANNELS**-0.5
        self.k = k_ref[rows, :].astype(F32)
        self.vs = heads_on_rows(v_ref[rows, :])
        self.g = dot_exact(lower, fd_ref[rows, :])
        self.h = dot_exact(upper, bd_ref[rows, :])
        self.last = self.g[BLOCK - 1 :, :]
        self.first = self.h[:1, :]
        self.mid_g = self.g[BLOCK // 2 - 1 : BLOCK // 2, :]
        self.mid_h = self.h[BLOCK // 2 : BLOCK // 2 + 1, :]

    def ends(self):
        self.eg_end = jnp.exp(self.last - self.g)
        self.eh_end = jnp.exp(self.first - self.h)
        self.kg_end = stacked(self.k * self.eg_end).astype(BF16)
        self.kh_end = stacked(self.k * self.eh_end).astype(BF16)
        self.fresh_f = dot(self.vs, self.kg_end, TN)
        self.fresh_b = dot(self.vs, self.kh_end, TN)

    def entries(self):
        self.eg = jnp.exp(self.g)
        self.eh = jnp.exp(self.h)
        self.qg = stacked(self.q * self.eg).astype(BF16)
        self.qh = stacked(self.q * self.eh).astype(BF16)

    def scores(self, inclusive, strict):
        self.up_g = jnp.exp(self.g - self.mid_g)
        self.dn_g = jnp.exp(self.mid_g - self.g)
        self.up_h = jnp.exp(self.h - self.mid_h)
        self.dn_h = jnp.exp(self.mid_h - self.h)
        self.q_up_g = stacked(self.q * self.up_g).astype(BF16)
        self.k_dn_g = stacked(self.k * self.dn_g).astype(BF16)
        self.q_up_h = stacked(self.q * self.up_h).astype(BF16)
        self.k_dn_h = stacked(self.k * self.dn_h).astype(BF16)
        a_f = jnp.where(inclusive, dot(self.q_up_g, self.k_dn_g, NT), 0.0)
        a_b = jnp.where(strict, dot(self.q_up_h, self.k_dn_h, NT), 0.0)
        return (a_f + a_b).astype(BF16)


def both_states(pieces, forward_entry, backward_entry):
    s, before = forward_entry, []
    for piece in pieces:
        before.append(s)
        s = jnp.exp(piece.last) * s + piece.fresh_f
    r, after = backward_entry, [None] * len(pieces)
    for b in reversed(range(len(pieces))):
        after[b] = r
        r = jnp.exp(pieces[b].first) * r + pieces[b].fresh_b
    return before, after, s, r


def position():
    z, y, c = (lax.axis_index(a) for a in SP)
    return z, y, c, y * 2 + c


def plane_peer(p, d, planes):
    other = lax.rem(p + d, planes)
    return other, {"sp_1": other // 2, "sp_2": lax.rem(other, 2)}


def greet(planes, depth):
    z, _, _, p = position()
    barrier = pltpu.get_barrier_semaphore()
    for d in range(1, planes):
        _, device = plane_peer(p, d, planes)
        pl.semaphore_signal(barrier, 1, device_id=device, device_id_type=pl.DeviceIdType.MESH)
    for d in range(1, depth):
        device = {"sp_0": lax.rem(z + d, depth)}
        pl.semaphore_signal(barrier, 1, device_id=device, device_id_type=pl.DeviceIdType.MESH)
    return barrier, planes + depth - 2


class Carry:
    SCRATCH_PLANES, SCRATCH_DEPTH = 8, 8

    @classmethod
    def scratch(cls):
        n, m = cls.SCRATCH_PLANES, cls.SCRATCH_DEPTH
        return [
            pltpu.VMEM((n, 2, ROWS, 128), F32),
            pltpu.VMEM((n, 2, ROWS, 128), F32),
            pltpu.VMEM((2, ROWS, 128), F32),
            pltpu.VMEM((m, ROWS, 128), F32),
            pltpu.VMEM((n, 2, PIECE, 128), F32),
            pltpu.VMEM((n, 2, PIECE, 128), F32),
            pltpu.SemaphoreType.DMA((n,)),
            pltpu.SemaphoreType.DMA((n,)),
            pltpu.SemaphoreType.DMA((m,)),
            pltpu.SemaphoreType.DMA((m,)),
            pltpu.SemaphoreType.DMA((n,)),
            pltpu.SemaphoreType.DMA((n,)),
        ]

    def __init__(self, refs):
        (
            self.out1,
            self.in1,
            self.out2,
            self.in2,
            self.out3,
            self.in3,
            self.s1,
            self.r1,
            self.s2,
            self.r2,
            self.s3,
            self.r3,
        ) = refs
        self.n, self.m = self.SCRATCH_PLANES, self.SCRATCH_DEPTH
        self.z, _, _, self.p = position()

    def plane_copy(self, out, into, send, recv, d, arriving=False):
        other, device = plane_peer(self.p, d, self.n)
        at = other if arriving else self.p
        return pltpu.make_async_remote_copy(
            src_ref=out.at[other],
            dst_ref=into.at[at],
            send_sem=send.at[other],
            recv_sem=recv.at[at],
            device_id=device,
            device_id_type=pl.DeviceIdType.MESH,
        )

    def start(self, terms, logs):
        for dim in range(2):
            decay = jnp.broadcast_to(logs[dim], (8, 128))
            for j in range(self.n):
                self.out1[j, dim, :PIECE, :] = terms[dim][j * PIECE : (j + 1) * PIECE, :]
                self.out1[j, dim, PIECE:, :] = decay
        for d in range(1, self.n):
            self.plane_copy(self.out1, self.in1, self.s1, self.r1, d).start()
        self.in1[self.p] = self.out1[self.p]

    def middle(self):
        for d in range(1, self.n):
            self.plane_copy(self.out1, self.in1, self.s1, self.r1, d, True).wait_recv()
        zero = jnp.zeros((PIECE, 128), F32)
        none = jnp.zeros((1, 128), F32)
        self.before = [[None] * self.n, [None] * self.n]
        for dim in range(2):
            total, log = zero, none
            for i in range(self.n) if dim == 0 else reversed(range(self.n)):
                self.before[dim][i] = (total, log)
                step = self.in1[i, dim, PIECE : PIECE + 1, :]
                total = total * jnp.exp(step) + self.in1[i, dim, :PIECE, :]
                log = log + step
            self.out2[dim, :PIECE, :] = total
            self.out2[dim, PIECE:, :] = jnp.broadcast_to(log, (8, 128))
        for d in range(1, self.m):
            self.depth_copy(d).start()

    def depth_copy(self, d, arriving=False):
        other = lax.rem(self.z + d, self.m)
        dim = jnp.where(other > self.z, 0, 1)
        at = other if arriving else self.z
        return pltpu.make_async_remote_copy(
            src_ref=self.out2.at[dim],
            dst_ref=self.in2.at[at],
            send_sem=self.s2.at[other],
            recv_sem=self.r2.at[at],
            device_id={"sp_0": other},
            device_id_type=pl.DeviceIdType.MESH,
        )

    def last(self):
        self.in2[self.z] = jnp.zeros((ROWS, 128), F32)
        for d in range(1, self.m):
            self.depth_copy(d, True).wait_recv()
        entry = []
        for dim in range(2):
            total = jnp.zeros((PIECE, 128), F32)
            for i in range(self.m) if dim == 0 else reversed(range(self.m)):
                passed = (i < self.z) if dim == 0 else (i > self.z)
                step = self.in2[i, PIECE : PIECE + 1, :]
                total = jnp.where(passed, total * jnp.exp(step) + self.in2[i, :PIECE, :], total)
            entry.append(total)
        for i in range(self.n):
            for dim in range(2):
                inside, log = self.before[dim][i]
                self.out3[i, dim] = inside + jnp.exp(log) * entry[dim]
        for d in range(1, self.n):
            self.plane_copy(self.out3, self.in3, self.s3, self.r3, d).start()
        self.in3[self.p] = self.out3[self.p]

    def finish(self):
        for d in range(1, self.n):
            self.plane_copy(self.out3, self.in3, self.s3, self.r3, d, True).wait_recv()
        for d in range(1, self.n):
            self.plane_copy(self.out1, self.in1, self.s1, self.r1, d).wait_send()
            self.plane_copy(self.out3, self.in3, self.s3, self.r3, d).wait_send()
        for d in range(1, self.m):
            self.depth_copy(d).wait_send()
        return [self.in3[:, dim].reshape(128, 128) for dim in range(2)]


def forward_kernel(q, k, v, fd, bd, o_ref, rows_ref, entry_ref, *scratch):
    barrier, count = greet(8, 8)
    pieces = [Piece(b, q, k, v, fd, bd) for b in range(3)]
    for piece in pieces:
        piece.ends()
    zero = jnp.zeros((DV, 128), F32)
    _, _, forward_end, backward_end = both_states(pieces, zero, zero)
    log_f = sum(piece.last for piece in pieces)
    log_b = sum(piece.first for piece in pieces)
    pl.semaphore_wait(barrier, count)
    carry = Carry(scratch)
    carry.start((forward_end, backward_end), (log_f, log_b))
    inclusive, strict = masks()
    inner = []
    for piece in pieces:
        inner.append(dot(piece.scores(inclusive, strict), piece.vs))
        piece.entries()
    carry.middle()
    carry.last()
    forward_entry, backward_entry = carry.finish()
    entry_ref[0] = forward_entry
    entry_ref[1] = backward_entry
    before, after, _, _ = both_states(pieces, forward_entry, backward_entry)
    for b, piece in enumerate(pieces):
        left = jnp.concatenate([piece.qg, piece.qh], axis=1)
        right = jnp.concatenate([before[b], after[b]], axis=1)
        o = inner[b] + dot(left, right, NT)
        o_ref[b] = o
        mixed = o * lax.rsqrt(jnp.mean(o * o, axis=1, keepdims=True) + EPSILON)
        rows_ref[pl.ds(b * BLOCK, BLOCK), :] = heads_on_lanes(mixed).astype(BF16)


def backward_kernel(
    stream, out_proj, q, k, v, fd, bd, o_ref, entry_ref, dq_ref, dk_ref, dv_ref, *scratch
):
    barrier, count = greet(8, 8)
    pieces = [Piece(b, q, k, v, fd, bd) for b in range(3)]
    mixed_grad = jnp.dot(stream[...], out_proj[...], preferred_element_type=F32)
    c, d = jnp.zeros((DV, 128), F32), jnp.zeros((DV, 128), F32)
    for b, piece in enumerate(pieces):
        o = o_ref[b]
        inv = lax.rsqrt(jnp.mean(o * o, axis=1, keepdims=True) + EPSILON)
        mixed = o * inv
        mg = heads_on_rows(mixed_grad[b * BLOCK : (b + 1) * BLOCK, :])
        piece.do = (inv * (mg - mixed * jnp.mean(mg * mixed, axis=1, keepdims=True))).astype(BF16)
        piece.entries()
        piece.back_f = dot(piece.do, piece.qg, TN)
        piece.back_b = dot(piece.do, piece.qh, TN)
    for piece in pieces:
        c = c * jnp.exp(piece.first) + piece.back_b
    for piece in reversed(pieces):
        d = d * jnp.exp(piece.last) + piece.back_f
    log_f = sum(piece.last for piece in pieces)
    log_b = sum(piece.first for piece in pieces)
    pl.semaphore_wait(barrier, count)
    carry = Carry(scratch)
    carry.start((c, d), (log_b, log_f))
    inclusive, strict = masks()
    for piece in pieces:
        a = piece.scores(inclusive, strict)
        da = dot(piece.do, piece.vs, NT)
        da_f = jnp.where(inclusive, da, 0.0).astype(BF16)
        da_b = jnp.where(strict, da, 0.0).astype(BF16)
        piece.dv = dot(a, piece.do, TN)
        piece.dq = dot(da_f, piece.k_dn_g) * doubled(piece.up_g) + dot(
            da_b, piece.k_dn_h
        ) * doubled(piece.up_h)
        piece.dk = dot(da_f, piece.q_up_g, TN) * doubled(piece.dn_g) + dot(
            da_b, piece.q_up_h, TN
        ) * doubled(piece.dn_h)
    carry.middle()
    for piece in pieces:
        piece.ends()
    before, after, _, _ = both_states(pieces, entry_ref[0], entry_ref[1])
    for b, piece in enumerate(pieces):
        dq = dot(piece.do, jnp.concatenate([before[b], after[b]], axis=1))
        piece.dq = piece.dq + dq[:, :128] * stacked(piece.eg) + dq[:, 128:] * stacked(piece.eh)
        dq_ref[pl.ds(b * BLOCK, BLOCK), :] = (folded(piece.dq) * KEY_CHANNELS**-0.5).astype(BF16)
    carry.last()
    c, d = carry.finish()
    late, early = [None] * 3, [None] * 3
    for b, piece in enumerate(pieces):
        early[b] = c
        c = c * jnp.exp(piece.first) + piece.back_b
    for b in reversed(range(3)):
        late[b] = d
        d = d * jnp.exp(pieces[b].last) + pieces[b].back_f
    for b, piece in enumerate(pieces):
        states = jnp.concatenate([late[b], early[b]], axis=1).astype(BF16)
        dk = dot(piece.vs, states)
        dk = piece.dk + dk[:, :128] * stacked(piece.eg_end) + dk[:, 128:] * stacked(piece.eh_end)
        dv = piece.dv + dot(jnp.concatenate([piece.kg_end, piece.kh_end], axis=1), states, NT)
        rows = pl.ds(b * BLOCK, BLOCK)
        dk_ref[rows, :] = folded(dk).astype(BF16)
        dv_ref[rows, :] = heads_on_lanes(dv).astype(BF16)


def vmem(n):
    return [pl.BlockSpec(memory_space=pltpu.VMEM)] * n


def attention_forward(q, k, v, fd, bd):
    tokens = q.shape[0]
    return pl.pallas_call(
        forward_kernel,
        out_shape=(
            jax.ShapeDtypeStruct((3, 128, DV), F32),
            jax.ShapeDtypeStruct((tokens, 2 * DV), BF16),
            jax.ShapeDtypeStruct((2, DV, 128), F32),
        ),
        in_specs=vmem(5),
        out_specs=tuple(vmem(3)),
        scratch_shapes=Carry.scratch(),
        compiler_params=pltpu.CompilerParams(collective_id=0, has_side_effects=True),
        cost_estimate=pl.CostEstimate(
            flops=10**9, bytes_accessed=2**20, transcendentals=0
        ),
        name="attention_forward",
    )(q, k, v, fd, bd)


def attention_backward(stream, out_proj, q, k, v, fd, bd, o, entry):
    tokens = q.shape[0]
    return pl.pallas_call(
        backward_kernel,
        out_shape=(
            jax.ShapeDtypeStruct((tokens, 128), BF16),
            jax.ShapeDtypeStruct((tokens, 128), BF16),
            jax.ShapeDtypeStruct((tokens, 2 * DV), BF16),
        ),
        in_specs=vmem(9),
        out_specs=tuple(vmem(3)),
        scratch_shapes=Carry.scratch(),
        compiler_params=pltpu.CompilerParams(collective_id=1, has_side_effects=True),
        cost_estimate=pl.CostEstimate(
            flops=10**9, bytes_accessed=2**21, transcendentals=0
        ),
        name="attention_backward",
    )(stream, out_proj, q, k, v, fd, bd, o, entry)


def copy_for_each(array, axis):
    devices = lax.axis_size(axis)
    return lax.all_to_all(
        jnp.broadcast_to(array[None], (devices, *array.shape)), axis, 0, 0, tiled=True
    )


def in_order(pieces, dim):
    shape = list(pieces.shape[1:])
    shape[dim] *= pieces.shape[0]
    return jnp.moveaxis(pieces, 0, dim).reshape(shape)


def slot_choice(routes, weights, experts, slots):
    tokens = routes.shape[0]
    ids = routes.reshape(-1)
    members = (ids[:, None] == jnp.arange(experts, dtype=jnp.int32)[None, :]).astype(BF16)
    earlier = jnp.tril(jnp.ones((2 * tokens, 2 * tokens), BF16), -1)
    before = jnp.dot(earlier, members, preferred_element_type=F32)
    ranks = jnp.sum(before * members.astype(F32), axis=1).astype(jnp.int32)
    target = jnp.where(ranks < CAP, ids * CAP + ranks, -1).reshape(tokens, 2)
    slot = jnp.arange(slots, dtype=jnp.int32)[:, None]
    first = slot == target[:, 0][None, :]
    second = slot == target[:, 1][None, :]
    chosen = (first | second).astype(BF16)
    weight = jnp.sum(
        jnp.where(first, weights[:, 0][None, :], 0.0)
        + jnp.where(second, weights[:, 1][None, :], 0.0),
        axis=1,
        keepdims=True,
    )
    return chosen, weight


def on_device(
    layer_grad,
    routes,
    route_weight,
    slot_tokens,
    gate_proj,
    up_proj,
    down_proj,
    out_proj,
    queries,
    keys,
    values,
    fwd_decay,
    bwd_decay,
):
    devices = lax.axis_size(SP)
    width = layer_grad.shape[1]
    slots = slot_tokens.shape[1]
    capacity = slots // devices
    quarter = width // lax.axis_size("tp")
    chosen, weight = slot_choice(routes, route_weight, devices, slots)
    own_columns = lax.dynamic_slice_in_dim(layer_grad, lax.axis_index("tp") * quarter, quarter, 1)
    outgoing = (jnp.dot(chosen, own_columns, preferred_element_type=F32) * weight).astype(BF16)
    arrived = lax.all_to_all(
        outgoing.reshape(devices, capacity, quarter), SP, split_axis=0, concat_axis=0, tiled=True
    ).reshape(slots, quarter)
    o, mixed_rows, entry = attention_forward(queries, keys, values, fwd_decay, bwd_decay)
    inbound = in_order(copy_for_each(arrived, "tp"), 1)
    inputs = slot_tokens[0]
    w_gate = gate_proj[0]
    w_upper = up_proj[0]
    w_down = down_proj[0]
    gate = jnp.dot(inputs, w_gate, preferred_element_type=F32)
    upper = jnp.dot(inputs, w_upper, preferred_element_type=F32)
    sigma = jax.nn.sigmoid(gate)
    act = (gate * sigma * upper).astype(BF16)
    grad_down = lax.dot_general(act, inbound, (TN, ((), ())), preferred_element_type=F32)
    act_grad = lax.dot_general(inbound, w_down, (NT, ((), ())), preferred_element_type=F32)
    up_delta = (act_grad * gate * sigma).astype(BF16)
    gate_delta = (act_grad * upper * sigma * (1.0 + gate * (1.0 - sigma))).astype(BF16)
    slot_part = lax.dot_general(gate_delta, w_gate, (NT, ((), ())), preferred_element_type=F32)
    slot_part = slot_part + lax.dot_general(
        up_delta, w_upper, (NT, ((), ())), preferred_element_type=F32
    )
    summed = lax.psum_scatter(slot_part.astype(BF16), "tp", scatter_dimension=1, tiled=True)
    grad_gate = lax.dot_general(inputs, gate_delta, (TN, ((), ())), preferred_element_type=F32)
    grad_up = lax.dot_general(inputs, up_delta, (TN, ((), ())), preferred_element_type=F32)
    backrows = lax.all_to_all(
        summed.reshape(devices, capacity, quarter), SP, split_axis=0, concat_axis=0, tiled=True
    ).reshape(slots, quarter)
    moe_grad = lax.dot_general(chosen, backrows, (TN, ((), ())), preferred_element_type=F32)
    stream_part = (own_columns.astype(F32) + moe_grad).astype(BF16)
    stream_grad = lax.all_gather(stream_part, "tp", axis=1, tiled=True)
    terms = lax.dot_general(
        stream_grad, mixed_rows, (TN, ((), ())), preferred_element_type=F32
    ).astype(BF16)
    arrived_terms = lax.all_to_all(
        terms.reshape(devices, -1, terms.shape[1]), SP, split_axis=0, concat_axis=0, tiled=True
    )
    proj_grad = arrived_terms.astype(F32).sum(axis=0)
    query_grad, key_grad, value_grad = attention_backward(
        stream_grad, out_proj, queries, keys, values, fwd_decay, bwd_decay, o, entry
    )
    return (
        grad_gate.astype(BF16)[None],
        grad_up.astype(BF16)[None],
        grad_down.astype(BF16)[None],
        proj_grad,
        query_grad,
        key_grad,
        value_grad,
    )


def solution(mesh):
    torus = Mesh(mesh.devices.reshape(8, 4, 2, mesh.shape["tp"]), ("sp_0", "sp_1", "sp_2", "tp"))
    in_specs = (
        P(SP, None),
        P(SP, None),
        P(SP, None),
        P(SP, None, None),
        P(SP, None, "tp"),
        P(SP, None, "tp"),
        P(SP, "tp", None),
        P(None, "tp"),
        P(SP, "tp"),
        P(SP, "tp"),
        P(SP, "tp"),
        P(SP, "tp"),
        P(SP, "tp"),
    )
    out_specs = (
        P(SP, None, "tp"),
        P(SP, None, "tp"),
        P(SP, "tp", None),
        P(SP, "tp"),
        P(SP, "tp"),
        P(SP, "tp"),
        P(SP, "tp"),
    )
    return jax.shard_map(
        on_device, mesh=torus, in_specs=in_specs, out_specs=out_specs, check_vma=False
    )
```

time: 502 us -> 256 us (0.51)
  blocking collectives: 157 us -> 52.1 us
  local copies, waits for them, and re-layouts: 119 us -> 20.8 us
  Pallas kernels: 0 us -> 64.2 us
  matrix products: 84.1 us -> 20.6 us
  other arithmetic: 47.3 us -> 3.06 us
  waiting for transfers between devices: 19.6 us -> 55.5 us
  starting transfers between devices: 52.6 us -> 24.1 us
    all_gather x12 -> x0, blocking collectives: 146 us -> none  [all_in_one(): both, at, found = (lax.all_gather(jnp.concatenate(lines), axis), 0, {})]
    pallas_call x0 -> x2, Pallas kernels: none -> 64.2 us  [the longest x1 37.7 us: attention_forward(): pl.pallas_call(forward_kernel, out_shape=(jax.ShapeDtypeStruct((3, 128, D...]
    dot_general x88 -> x12, matrix products: 84.1 us -> 20.6 us  [the longest x1 4.04 us: on_device(): lax.dot_general(act, inbound, (TN, ((), ())), preferred_element_type=F32)]
    all_to_all x0 -> x1, blocking collectives: none -> 41.2 us  [on_device(): lax.all_to_all(outgoing.reshape(devices, capacity, quarter), SP, split_ax...]
    reduce_scatter x1, waiting for transfers between devices: 0.01 us -> 30.6 us  [on_device(): lax.psum_scatter(slot_part.astype(BF16), 'tp', scatter_dimension=1, tiled...]
    all_to_all x1, waiting for transfers between devices: 5.6 us -> 24.9 us  [copy_for_each(): lax.all_to_all(jnp.broadcast_to(array[None], (devices, *array.shape)), ax...]
    all_to_all x2 -> x1, starting transfers between devices: 27.4 us -> 8.67 us  [on_device(): lax.all_to_all(terms.reshape(devices, -1, terms.shape[1]), SP, split_axis...]
    mul x42 -> x1, local copies, waits for them, and re-layouts: 16.8 us -> 0.11 us  [slot_choice(): target = jnp.where(ranks < CAP, ids * CAP + ranks, -1).reshape(tokens, 2)]
  transfers between devices with their start and end apart: 5 -> 4, of which waited for: 2 -> 2; matrix products, arithmetic and copies ran while one was open for 38% -> 5% of each run, Pallas kernels for 0% -> 25%
where the time goes in v1:
time: 256 us; the launch traced here: 255 us
  Pallas kernels  64.2 us (25%)
  waiting for transfers between devices  55.5 us (22%)
  blocking collectives  52.1 us (20%)
  starting transfers between devices  24.1 us (9%)
  local copies, waits for them, and re-layouts  20.8 us (8%)
  matrix products  20.6 us (8%)
  between operations  14.3 us (6%)
  other arithmetic  3.06 us (1%)
    all_to_all x1, blocking collectives, on_device(): lax.all_to_all(outgoing.reshape(devices, capacity, quarter), SP, split_ax...  41.2 us
    pallas_call x1, Pallas kernels, attention_forward(): pl.pallas_call(forward_kernel, out_shape=(jax.ShapeDtypeStruct((3, 128, D...  37.7 us
    reduce_scatter x1, waiting for transfers between devices, on_device(): lax.psum_scatter(slot_part.astype(BF16), 'tp', scatter_dimension=1, tiled...  30.6 us
    pallas_call x1, Pallas kernels, attention_backward(): pl.pallas_call(backward_kernel, out_shape=(jax.ShapeDtypeStruct((tokens,...  26.6 us
    all_to_all x1, waiting for transfers between devices, copy_for_each(): lax.all_to_all(jnp.broadcast_to(array[None], (devices, *array.shape)), ax...  24.9 us
    all_gather x1, blocking collectives, on_device(): stream_grad = lax.all_gather(stream_part, 'tp', axis=1, tiled=True)  10.9 us
    all_to_all x1, starting transfers between devices, on_device(): lax.all_to_all(summed.reshape(devices, capacity, quarter), SP, split_axis...  10.7 us
    unnamed x30, local copies, waits for them, and re-layouts  9.76 us
  transfers between devices with their start and end apart: 4, of which 2 were waited for; matrix products, arithmetic and copies ran while one was open for 5% of the time, Pallas kernels for 25%

profile of v1, /device:TPU:1, one launch (start us, length us, event | category | flops | bytes accessed | tf_op | source)
XLA Modules:
  0.0 254.8 jit_solution(7150042246520661010)
XLA Ops:
  10.8 2.2 fusion.9
  14.3 41.2 %all_to_all.20 = bf16[64,9,512]{2,1,0:T(8,128)(2,1)} all-to-all(bf16[64,9,512]{2,1,0:T(8,128)(2,1)S(1)} %reshape.40), channel_id=1, replica_groups=mesh['sp_0'=8,'sp_1'=4,'sp_2'=2,'tp'=4] {'sp_0','sp_1','sp_2'}, dimensions={0} | all-to-all | bytes 1179648 | tf_op jit(solution)/shard_map/all_to_all | solution.py:477
  55.5 1.4 broadcast_in_dim.60
  57.0 1.6 broadcast_in_dim.61
  58.6 4.7 %all-to-all-start.1 = ((bf16[4,576,512]{2,1,0:T(8,128)(2,1)}), bf16[4,576,512]{2,1,0:T(8,128)(2,1)}, u32[]{:S(2)}, u32[]{:S(2)}) async-start(bf16[4,576,512]{2,1,0:T(8,128)(2,1)} %broadcast_in_dim.61), calls=%async_computation.1 | async-start | bytes 4718592 | tf_op jit(solution)/shard_map/all_to_all | solution.py:422
  63.3 1.6 fusion.5
  64.9 1.6 fusion.7
  66.5 24.9 %all-to-all-done.1 = bf16[4,576,512]{2,1,0:T(8,128)(2,1)} async-done(((bf16[4,576,512]{2,1,0:T(8,128)(2,1)}), bf16[4,576,512]{2,1,0:T(8,128)(2,1)}, u32[]{:S(2)}, u32[]{:S(2)}) %all-to-all-start.1) | async-done | bytes 2359328 | tf_op jit(solution)/shard_map/all_to_all | solution.py:422
  91.4 2.1 copy.44
  96.3 2.2 add_convert_fusion
  98.6 30.6 %reduce-scatter.2.cloned.1.call-done = bf16[576,512]{1,0:T(8,128)(2,1)} async-done(((bf16[576,2048]{1,0:T(8,128)(2,1)}), bf16[576,512]{1,0:T(8,128)(2,1)}) %reduce-scatter.2.cloned.1.call-update) | async-done | bytes 589840 | tf_op jit(solution)/shard_map/reduce_scatter | solution.py:498
  129.2 2.2 reshape.42
  131.4 10.7 %all-to-all-start.2 = ((bf16[64,9,512]{2,1,0:T(8,128)(2,1)}), bf16[64,9,512]{2,1,0:T(8,128)(2,1)S(1)}, u32[]{:S(2)}, u32[]{:S(2)}) async-start(bf16[64,9,512]{2,1,0:T(8,128)(2,1)} %reshape.42), calls=%async_computation.3 | async-start | bytes 2097152 | tf_op jit(solution)/shard_map/all_to_all | solution.py:501
  142.1 37.7 %attention_forward.1 = (f32[3,128,128]{2,1,0:T(8,128)}, bf16[192,256]{1,0:T(8,128)(2,1)}, f32[2,128,128]{2,1,0:T(8,128)}) custom-call(bf16[192,128]{1,0:T(8,128)(2,1)} %q.3, bf16[192,128]{1,0:T(8,128)(2,1)} %k.3, bf16[192,256]{1,0:T(8,128)(2,1)} %v.3, f32[192,128]{1,0:T(8,128)} %fd.3, f32[192,128]{1,0:T(8,128)} %bd.3), custom_call_target="tpu_custom_call" | custom-call | flops 1000000000 | bytes 1048576 | tf_op jit(solution)/shard_map/attention_forward/pallas_call | solution.py:382
  180.9 1.5 fusion.10
  182.4 10.9 %all_gather.3.stream = bf16[192,2048]{1,0:T(8,128)(2,1)S(1)} all-gather(bf16[192,512]{1,0:T(8,128)(2,1)S(1)} %fusion.10), channel_id=1, replica_groups=mesh['sp_0'=8,'sp_1'=4,'sp_2'=2,'tp'=4] {'tp'}, dimensions={1}, use_global_device_ids=true | all-gather | bytes 983040 | tf_op jit(solution)/shard_map/all_gather | solution.py:506
  194.2 1.5 convolution_convert_fusion.3
  195.7 8.7 %all-to-all-start.3 = ((bf16[64,32,256]{2,1,0:T(8,128)(2,1)}), bf16[64,32,256]{2,1,0:T(8,128)(2,1)}, u32[]{:S(2)}, u32[]{:S(2)}) async-start(bf16[64,32,256]{2,1,0:T(8,128)(2,1)} %bitcast.12), calls=%async_computation.4 | async-start | bytes 2097152 | tf_op jit(solution)/shard_map/all_to_all | solution.py:510
  204.4 2.0 fusion
  207.6 2.0 fusion.1
  210.9 4.0 %fusion.2 = bf16[1,256,2048]{2,1,0:T(8,128)(2,1)} fusion(bf16[576,2048]{1,0:T(8,128)(2,1)} %bitcast.50, f32[576,256]{1,0:T(8,128)} %fusion.7, f32[576,256]{1,0:T(8,128)} %fusion.5), kind=kOutput, calls=%fused_computation.7 | convolution fusion | flops 605388800 | bytes 4587520 | tf_op jit(solution)/shard_map/dot_general | solution.py:490
  214.9 26.6 %attention_backward.1 = (bf16[192,128]{1,0:T(8,128)(2,1)}, bf16[192,128]{1,0:T(8,128)(2,1)}, bf16[192,256]{1,0:T(8,128)(2,1)}) custom-call(bf16[192,2048]{1,0:T(8,128)(2,1)} %copy-done.2, bf16[2048,256]{1,0:T(8,128)(2,1)} %out_proj.1, bf16[192,128]{1,0:T(8,128)(2,1)} %q.3, bf16[192,128]{1,0:T(8,128)(2,1)} %k.3, bf16[192,256]{1,0:T(8,128)(2,1)} %v.3, ...), custom_call_target="tpu_custom_call" | custom-call | flops 1000000000 | bytes 2097152 | tf_op jit(solution)/shard_map/attention_backward/pallas_call | solution.py:402
  241.5 2.0 convert_reduce_fusion
  246.4 1.5 copy.50
  (48 shorter events, 15.1 us)
Async XLA Ops:
  7.2 56.1 %copy-start = (bf16[1,576,2048]{2,1,0:T(8,128)(2,1)S(1)}, bf16[1,576,2048]{2,1,0:T(8,128)(2,1)}, u32[]{:S(2)}) copy-start(bf16[1,576,2048]{2,1,0:T(8,128)(2,1)} %param.16) | copy-start | bytes 7077892
  58.6 4.7 %copy-start.5 = (bf16[1,2048,256]{2,1,0:T(8,128)(2,1)S(1)}, bf16[1,2048,256]{2,1,0:T(8,128)(2,1)}, u32[]{:S(2)}) copy-start(bf16[1,2048,256]{2,1,0:T(8,128)(2,1)} %param.17) | copy-start | bytes 3145732
  58.6 32.8 %all-to-all-start.1 = ((bf16[4,576,512]{2,1,0:T(8,128)(2,1)}), bf16[4,576,512]{2,1,0:T(8,128)(2,1)}, u32[]{:S(2)}, u32[]{:S(2)}) async-start(bf16[4,576,512]{2,1,0:T(8,128)(2,1)} %broadcast_in_dim.61), calls=%async_computation.1 | async-start | bytes 4718592 | tf_op jit(solution)/shard_map/all_to_all | solution.py:422
  63.2 66.0 %reduce-scatter.2.cloned.1.call-start = ((), (), s32[]{:S(2)}) async-start(), calls=%async_computation.5 | async-start | bytes 2949120 | tf_op jit(solution)/shard_map/reduce_scatter | solution.py:498
  63.3 1.6 copy-start.6
  91.4 2.1 copy-start.8
  91.4 2.1 copy-start.9
  91.4 2.3 copy-start.11
  93.5 1.4 copy-start.1
  94.9 0.8 copy-start.3
  94.9 0.8 copy-start.4
  94.9 1.4 copy-start.7
  131.4 48.4 %all-to-all-start.2 = ((bf16[64,9,512]{2,1,0:T(8,128)(2,1)}), bf16[64,9,512]{2,1,0:T(8,128)(2,1)S(1)}, u32[]{:S(2)}, u32[]{:S(2)}) async-start(bf16[64,9,512]{2,1,0:T(8,128)(2,1)} %reshape.42), calls=%async_computation.3 | async-start | bytes 2097152 | tf_op jit(solution)/shard_map/all_to_all | solution.py:501
  179.8 14.4 %copy-start.10 = (bf16[192,256]{1,0:T(8,128)(2,1)S(1)}, bf16[192,256]{1,0:T(8,128)(2,1)}, u32[]{:S(2)}) copy-start(bf16[192,256]{1,0:T(8,128)(2,1)} %get-tuple-element.13) | copy-start | bytes 294916
  193.3 0.9 copy-start.2
  195.7 45.9 %all-to-all-start.3 = ((bf16[64,32,256]{2,1,0:T(8,128)(2,1)}), bf16[64,32,256]{2,1,0:T(8,128)(2,1)}, u32[]{:S(2)}, u32[]{:S(2)}) async-start(bf16[64,32,256]{2,1,0:T(8,128)(2,1)} %bitcast.12), calls=%async_computation.4 | async-start | bytes 2097152 | tf_op jit(solution)/shard_map/all_to_all | solution.py:510
Sparse Core Ops, SparseCore 0:
  98.7 30.4 reduce-scatter.1

commit v2 on v1

--- a/solution.py
+++ b/solution.py
@@ -1,5 +1,3 @@
-import functools
-
 import jax
 import jax.numpy as jnp
 from jax import lax
@@ -276,8 +274,120 @@
         return [self.in3[:, dim].reshape(128, 128) for dim in range(2)]
 
 
-def forward_kernel(q, k, v, fd, bd, o_ref, rows_ref, entry_ref, *scratch):
-    barrier, count = greet(8, 8)
+OFFSETS = (0, 1, 7, 2, 6, 3, 5, 4)
+PLANE_ORDER = (2, 6, 3, 7, 4, 5, 1)
+PLANES, DEPTH, RING = 8, 8, 4
+CHUNK = PLANES * CAP
+MESH = pl.DeviceIdType.MESH
+
+
+def remote(src, dst, sems, device):
+    return pltpu.make_async_remote_copy(
+        src_ref=src,
+        dst_ref=dst,
+        send_sem=sems[0],
+        recv_sem=sems[1],
+        device_id=device,
+        device_id_type=MESH,
+    )
+
+
+def swap_matrix(shape):
+    i = iota((shape[0], 1), 0)
+    a = (i * 911) >> 16
+    rest = i - a * CHUNK
+    b = (rest * 7282) >> 16
+    source = b * CHUNK + a * CAP + (rest - b * CAP)
+    return jnp.where(source == iota(shape, 1), 1.0, 0.0).astype(BF16)
+
+
+def expert_kernel(
+    chosen,
+    weight,
+    layer_grad,
+    slot_tokens,
+    gate_proj,
+    up_proj,
+    down_proj,
+    q,
+    k,
+    v,
+    fd,
+    bd,
+    stream_ref,
+    gate_grad_ref,
+    up_grad_ref,
+    down_grad_ref,
+    o_ref,
+    rows_ref,
+    entry_ref,
+    own,
+    x,
+    w_cat,
+    w_down,
+    swap,
+    act,
+    silu,
+    slope,
+    delta,
+    out_plane,
+    in_plane,
+    out_depth,
+    inbound,
+    part,
+    hop,
+    hopped,
+    both,
+    plain,
+    ret_out,
+    ret_in,
+    back_out,
+    back_in,
+    stream,
+    send,
+    recv,
+    load,
+    *carry_refs,
+):
+    z, _, _, p = position()
+    t = lax.axis_index("tp")
+    right, left, across = lax.rem(t + 1, RING), lax.rem(t + 3, RING), lax.rem(t + 2, RING)
+    quarter = own.shape[1]
+    barrier, count = greet(PLANES, DEPTH)
+    for other in (left, right):
+        pl.semaphore_signal(barrier, 1, device_id={"tp": other}, device_id_type=MESH)
+
+    columns = pl.ds(pl.multiple_of(t * quarter, quarter), quarter)
+    hidden = w_down.shape[0]
+    loads = [
+        pltpu.make_async_copy(layer_grad.at[:, columns], own, load.at[0]),
+        pltpu.make_async_copy(slot_tokens.at[0], x, load.at[1]),
+        pltpu.make_async_copy(gate_proj.at[0], w_cat.at[:, pl.ds(0, hidden)], load.at[2]),
+        pltpu.make_async_copy(up_proj.at[0], w_cat.at[:, pl.ds(hidden, hidden)], load.at[3]),
+        pltpu.make_async_copy(down_proj.at[0], w_down, load.at[4]),
+    ]
+    for copy in loads:
+        copy.start()
+
+    def sems(kind, i):
+        return send.at[kind, i], recv.at[kind, i]
+
+    def plane_out(kind, out, into, d):
+        other, device = plane_peer(p, d, PLANES)
+        return remote(out.at[other], into.at[p], sems(kind, d), device)
+
+    def plane_in(kind, out, into, d):
+        other, device = plane_peer(p, PLANES - d, PLANES)
+        return remote(out.at[other], into.at[other], sems(kind, d), device)
+
+    loads[0].wait()
+    picked = dot(chosen[...], own[...]) * weight[...]
+    out_plane[...] = picked.astype(BF16).reshape(out_plane.shape)
+    pl.semaphore_wait(barrier, count + 2)
+    for d in PLANE_ORDER:
+        plane_out(0, out_plane, in_plane, d).start()
+    in_plane[p] = out_plane[p]
+
     pieces = [Piece(b, q, k, v, fd, bd) for b in range(3)]
     for piece in pieces:
         piece.ends()
@@ -285,27 +395,212 @@
     _, _, forward_end, backward_end = both_states(pieces, zero, zero)
     log_f = sum(piece.last for piece in pieces)
     log_b = sum(piece.first for piece in pieces)
-    pl.semaphore_wait(barrier, count)
-    carry = Carry(scratch)
+    carry = Carry(carry_refs)
     carry.start((forward_end, backward_end), (log_f, log_b))
-    inclusive, strict = masks()
-    inner = []
-    for piece in pieces:
-        inner.append(dot(piece.scores(inclusive, strict), piece.vs))
-        piece.entries()
+    swap[...] = swap_matrix(swap.shape)
+
+    for d in PLANE_ORDER:
+        plane_in(0, out_plane, in_plane, d).wait_recv()
+    moved = dot(swap[...], in_plane[...].reshape(DEPTH * CHUNK, quarter)).astype(BF16)
+    out_depth[...] = moved.reshape(out_depth.shape)
     carry.middle()
-    carry.last()
-    forward_entry, backward_entry = carry.finish()
-    entry_ref[0] = forward_entry
-    entry_ref[1] = backward_entry
-    before, after, _, _ = both_states(pieces, forward_entry, backward_entry)
-    for b, piece in enumerate(pieces):
-        left = jnp.concatenate([piece.qg, piece.qh], axis=1)
-        right = jnp.concatenate([before[b], after[b]], axis=1)
-        o = inner[b] + dot(left, right, NT)
-        o_ref[b] = o
-        mixed = o * lax.rsqrt(jnp.mean(o * o, axis=1, keepdims=True) + EPSILON)
-        rows_ref[pl.ds(b * BLOCK, BLOCK), :] = heads_on_lanes(mixed).astype(BF16)
+
+    def depth_out(i):
+        other = lax.rem(z + DEPTH - OFFSETS[i], DEPTH)
+        return remote(out_depth.at[other], inbound.at[t, z], sems(1, i), {"sp_0": other})
+
+    for i in range(1, DEPTH):
+        depth_out(i).start()
+    inbound[t, z] = out_depth[z]
+
+    for copy in loads[1:4]:
+        copy.wait()
+    half = x.shape[0] // 2
+    for j in range(2):
+        rows = pl.ds(j * half, half)
+        chunks = pl.ds(j * (DEPTH // 2), DEPTH // 2)
+        both_up = jnp.dot(x[rows, :], w_cat[...], preferred_element_type=F32)
+        gate, up = both_up[:, :hidden], both_up[:, hidden:]
+        sigma = jax.nn.sigmoid(gate)
+        s = gate * sigma
+        shape = (DEPTH // 2, CHUNK, hidden)
+        silu[chunks] = s.reshape(shape)
+        act[chunks] = (s * up).astype(BF16).reshape(shape)
+        slope[chunks] = (up * sigma * (1.0 + gate * (1.0 - sigma))).reshape(shape)
+    loads[4].wait()
+
+    def chunk_of(i):
+        return lax.rem(z + OFFSETS[i], DEPTH)
+
+    def spread(i, arriving=False):
+        at = chunk_of(i)
+        a, b = (left, right) if arriving else (t, t)
+        return (
+            remote(inbound.at[a, at], inbound.at[a, at], sems(2, i), {"tp": right}),
+            remote(inbound.at[b, at], inbound.at[b, at], sems(3, i), {"tp": left}),
+        )
+
+    def sides(i):
+        return (left, right) if i % 2 == 0 else (right, left)
+
+    def pass_on(i, arriving=False):
+        source, to = sides(i)
+        at, which = chunk_of(i), across if arriving else source
+        return remote(inbound.at[which, at], inbound.at[which, at], sems(4, i), {"tp": to})
+
+    def send_hop(i):
+        _, to = sides(i)
+        return remote(part.at[i, across], hop.at[i], sems(5, i), {"tp": to})
+
+    def send_both(i):
+        _, to = sides(i)
+        return remote(hopped.at[i], both.at[i], sems(6, i), {"tp": to})
+
+    def send_plain(i):
+        to, _ = sides(i)
+        return remote(part.at[i, to], plain.at[i], sems(7, i), {"tp": to})
+
+    def send_back(i, arriving=False):
+        at = lax.rem(z + DEPTH - OFFSETS[i], DEPTH) if arriving else z
+        other = chunk_of(i)
+        return remote(ret_out.at[other], ret_in.at[at], sems(8, i), {"sp_0": other})
+
+    def stage_0(i):
+        if i > 0:
+            at = chunk_of(i)
+            remote(out_depth.at[at], inbound.at[t, at], sems(1, i), {"sp_0": at}).wait_recv()
+        for copy in spread(i):
+            copy.start()
+
+    def stage_1(i):
+        for copy in spread(i, True):
+            copy.wait_recv()
+        pass_on(i).start()
+
+    def stage_2(i):
+        at = chunk_of(i)
+        pass_on(i, True).wait_recv()
+        total = jnp.zeros((CHUNK, hidden), F32)
+        for n in range(RING):
+            total = total + dot(inbound[n, at], w_down[:, n * quarter : (n + 1) * quarter], NT)
+        up_delta = (total * silu[at]).astype(BF16)
+        gate_delta = (total * slope[at]).astype(BF16)
+        deltas = jnp.concatenate([gate_delta, up_delta], axis=1)
+        delta[at] = deltas
+        _, to = sides(i)
+        for n, which in enumerate((across, sides(i)[0], to, t)):
+            rows = pl.ds(pl.multiple_of(which * quarter, quarter), quarter)
+            part[i, which] = dot(deltas, w_cat[rows, :], NT).astype(BF16)
+            if n == 0:
+                send_hop(i).start()
+            if n == 1:
+                send_plain(i).start()
+
+    def stage_3(i):
+        _, to = sides(i)
+        send_hop(i).wait_recv()
+        hopped[i] = (hop[i].astype(F32) + part[i, to].astype(F32)).astype(BF16)
+        send_both(i).start()
+
+    def stage_4(i):
+        at = chunk_of(i)
+        send_both(i).wait_recv()
+        send_plain(i).wait_recv()
+        total = part[i, t].astype(F32) + both[i].astype(F32) + plain[i].astype(F32)
+        if i == 0:
+            ret_in[z] = total.astype(BF16)
+        else:
+            ret_out[at] = total.astype(BF16)
+            send_back(i).start()
+
+    stages = (stage_0, stage_1, stage_2, stage_3, stage_4)
+    for n in range(DEPTH + len(stages) - 1):
+        for lag, stage in enumerate(stages):
+            if 0 <= n - lag < DEPTH:
+                stage(n - lag)
+        if n == 0:
+            carry.last()
+        if n == 1:
+            inclusive, strict = masks()
+            inner = []
+            for piece in pieces:
+                inner.append(dot(piece.scores(inclusive, strict), piece.vs))
+                piece.entries()
+        if n == 3:
+            forward_entry, backward_entry = carry.finish()
+            entry_ref[0] = forward_entry
+            entry_ref[1] = backward_entry
+            before, after, _, _ = both_states(pieces, forward_entry, backward_entry)
+            for b, piece in enumerate(pieces):
+                across_state = jnp.concatenate([before[b], after[b]], axis=1)
+                o = inner[b] + dot(
+                    jnp.concatenate([piece.qg, piece.qh], axis=1), across_state, NT
+                )
+                o_ref[b] = o
+                mixed = o * lax.rsqrt(jnp.mean(o * o, axis=1, keepdims=True) + EPSILON)
+                rows_ref[pl.ds(b * BLOCK, BLOCK), :] = heads_on_lanes(mixed).astype(BF16)
+
+    act_all = act[...].reshape(DEPTH * CHUNK, hidden)
+    for n in range(RING):
+        rows = inbound[n].reshape(DEPTH * CHUNK, quarter)
+        down_grad_ref[:, n * quarter : (n + 1) * quarter] = dot(act_all, rows, TN).astype(BF16)
+
+    for i in range(1, DEPTH):
+        send_back(i, True).wait_recv()
+    moved = dot(swap[...], ret_in[...].reshape(DEPTH * CHUNK, quarter)).astype(BF16)
+    back_out[...] = moved.reshape(back_out.shape)
+    for d in PLANE_ORDER:
+        plane_out(9, back_out, back_in, d).start()
+    back_in[p] = back_out[p]
+    deltas = delta[...].reshape(DEPTH * CHUNK, 2 * hidden)
+    for n in range(RING):
+        both_grads = dot(x[:, n * quarter : (n + 1) * quarter], deltas, TN)
+        rows = pl.ds(n * quarter, quarter)
+        gate_grad_ref[rows, :] = both_grads[:, :hidden].astype(BF16)
+        up_grad_ref[rows, :] = both_grads[:, hidden:].astype(BF16)
+    for d in PLANE_ORDER:
+        plane_in(9, back_out, back_in, d).wait_recv()
+    moe_grad = dot(chosen[...], back_in[...].reshape(DEPTH * CHUNK, quarter), TN)
+    stream[t] = (own[...].astype(F32) + moe_grad).astype(BF16)
+
+    tokens = own.shape[0]
+
+    def stream_spread(arriving=False):
+        a, b = (left, right) if arriving else (t, t)
+        return (
+            remote(stream.at[a], stream.at[a], sems(0, 0), {"tp": right}),
+            remote(stream.at[b], stream.at[b], sems(1, 0), {"tp": left}),
+        )
+
+    def stream_pass(arriving=False):
+        top, low = pl.ds(0, tokens // 2), pl.ds(tokens // 2, tokens // 2)
+        a, b = (across, across) if arriving else (left, right)
+        return (
+            remote(stream.at[a, top], stream.at[a, top], sems(8, 0), {"tp": right}),
+            remote(stream.at[b, low], stream.at[b, low], sems(9, 0), {"tp": left}),
+        )
+
+    for copy in stream_spread():
+        copy.start()
+    for copy, onward in zip(stream_spread(True), stream_pass()):
+        copy.wait_recv()
+        onward.start()
+    for copy in stream_pass(True):
+        copy.wait_recv()
+    for n in range(RING):
+        stream_ref[:, n * quarter : (n + 1) * quarter] = stream[n]
+
+    for d in PLANE_ORDER:
+        plane_out(0, out_plane, in_plane, d).wait_send()
+        plane_out(9, back_out, back_in, d).wait_send()
+    for i in range(DEPTH):
+        if i > 0:
+            depth_out(i).wait_send()
+            send_back(i).wait_send()
+        for copy in (*spread(i), pass_on(i), send_hop(i), send_both(i), send_plain(i)):
+            copy.wait_send()
+    for copy in (*stream_spread(), *stream_pass()):
+        copy.wait_send()
 
 
 def backward_kernel(
@@ -377,24 +672,56 @@
     return [pl.BlockSpec(memory_space=pltpu.VMEM)] * n
 
 
-def attention_forward(q, k, v, fd, bd):
-    tokens = q.shape[0]
+def experts(chosen, weight, layer_grad, slot_tokens, gate, up, down, q, k, v, fd, bd):
+    tokens, width = layer_grad.shape
+    slots = slot_tokens.shape[1]
+    quarter = width // RING
+    hidden = gate.shape[2]
+    rows = (DEPTH, CHUNK, quarter)
+    anywhere = pl.BlockSpec(memory_space=pl.ANY)
     return pl.pallas_call(
-        forward_kernel,
+        expert_kernel,
         out_shape=(
+            jax.ShapeDtypeStruct((tokens, width), BF16),
+            jax.ShapeDtypeStruct((width, hidden), BF16),
+            jax.ShapeDtypeStruct((width, hidden), BF16),
+            jax.ShapeDtypeStruct((hidden, width), BF16),
             jax.ShapeDtypeStruct((3, 128, DV), F32),
             jax.ShapeDtypeStruct((tokens, 2 * DV), BF16),
             jax.ShapeDtypeStruct((2, DV, 128), F32),
         ),
-        in_specs=vmem(5),
-        out_specs=tuple(vmem(3)),
-        scratch_shapes=Carry.scratch(),
-        compiler_params=pltpu.CompilerParams(collective_id=0, has_side_effects=True),
+        in_specs=vmem(2) + [anywhere] * 5 + vmem(5),
+        out_specs=tuple(vmem(7)),
+        scratch_shapes=[
+            pltpu.VMEM((tokens, quarter), BF16),
+            pltpu.VMEM((slots, width), BF16),
+            pltpu.VMEM((width, 2 * hidden), BF16),
+            pltpu.VMEM((hidden, width), BF16),
+            pltpu.VMEM((slots, slots), BF16),
+            pltpu.VMEM((DEPTH, CHUNK, hidden), BF16),
+            pltpu.VMEM((DEPTH, CHUNK, hidden), F32),
+            pltpu.VMEM((DEPTH, CHUNK, hidden), F32),
+            pltpu.VMEM((DEPTH, CHUNK, 2 * hidden), BF16),
+            pltpu.VMEM(rows, BF16),
+            pltpu.VMEM(rows, BF16),
+            pltpu.VMEM(rows, BF16),
+            pltpu.VMEM((RING, *rows), BF16),
+            pltpu.VMEM((DEPTH, RING, CHUNK, quarter), BF16),
+            *[pltpu.VMEM(rows, BF16)] * 8,
+            pltpu.VMEM((RING, tokens, quarter), BF16),
+            pltpu.SemaphoreType.DMA((10, DEPTH)),
+            pltpu.SemaphoreType.DMA((10, DEPTH)),
+            pltpu.SemaphoreType.DMA((5,)),
+            *Carry.scratch(),
+        ],
+        compiler_params=pltpu.CompilerParams(
+            collective_id=0, has_side_effects=True, vmem_limit_bytes=60 * 2**20
+        ),
         cost_estimate=pl.CostEstimate(
-            flops=10**9, bytes_accessed=2**20, transcendentals=0
+            flops=6 * 10**9, bytes_accessed=10 * 2**20, transcendentals=0
         ),
-        name="attention_forward",
-    )(q, k, v, fd, bd)
+        name="experts",
+    )(chosen, weight, layer_grad, slot_tokens, gate, up, down, q, k, v, fd, bd)
 
 
 def attention_backward(stream, out_proj, q, k, v, fd, bd, o, entry):
@@ -417,19 +744,6 @@
     )(stream, out_proj, q, k, v, fd, bd, o, entry)
 
 
-def copy_for_each(array, axis):
-    devices = lax.axis_size(axis)
-    return lax.all_to_all(
-        jnp.broadcast_to(array[None], (devices, *array.shape)), axis, 0, 0, tiled=True
-    )
-
-
-def in_order(pieces, dim):
-    shape = list(pieces.shape[1:])
-    shape[dim] *= pieces.shape[0]
-    return jnp.moveaxis(pieces, 0, dim).reshape(shape)
-
-
 def slot_choice(routes, weights, experts, slots):
     tokens = routes.shape[0]
     ids = routes.reshape(-1)
@@ -438,7 +752,9 @@
     before = jnp.dot(earlier, members, preferred_element_type=F32)
     ranks = jnp.sum(before * members.astype(F32), axis=1).astype(jnp.int32)
     target = jnp.where(ranks < CAP, ids * CAP + ranks, -1).reshape(tokens, 2)
-    slot = jnp.arange(slots, dtype=jnp.int32)[:, None]
+    row = jnp.arange(slots, dtype=jnp.int32)
+    expert = (row // CAP) % DEPTH * PLANES + row // CHUNK
+    slot = (expert * CAP + row % CAP)[:, None]
     first = slot == target[:, 0][None, :]
     second = slot == target[:, 1][None, :]
     chosen = (first | second).astype(BF16)
@@ -467,43 +783,22 @@
     bwd_decay,
 ):
     devices = lax.axis_size(SP)
-    width = layer_grad.shape[1]
     slots = slot_tokens.shape[1]
-    capacity = slots // devices
-    quarter = width // lax.axis_size("tp")
     chosen, weight = slot_choice(routes, route_weight, devices, slots)
-    own_columns = lax.dynamic_slice_in_dim(layer_grad, lax.axis_index("tp") * quarter, quarter, 1)
-    outgoing = (jnp.dot(chosen, own_columns, preferred_element_type=F32) * weight).astype(BF16)
-    arrived = lax.all_to_all(
-        outgoing.reshape(devices, capacity, quarter), SP, split_axis=0, concat_axis=0, tiled=True
-    ).reshape(slots, quarter)
-    o, mixed_rows, entry = attention_forward(queries, keys, values, fwd_decay, bwd_decay)
-    inbound = in_order(copy_for_each(arrived, "tp"), 1)
-    inputs = slot_tokens[0]
-    w_gate = gate_proj[0]
-    w_upper = up_proj[0]
-    w_down = down_proj[0]
-    gate = jnp.dot(inputs, w_gate, preferred_element_type=F32)
-    upper = jnp.dot(inputs, w_upper, preferred_element_type=F32)
-    sigma = jax.nn.sigmoid(gate)
-    act = (gate * sigma * upper).astype(BF16)
-    grad_down = lax.dot_general(act, inbound, (TN, ((), ())), preferred_element_type=F32)
-    act_grad = lax.dot_general(inbound, w_down, (NT, ((), ())), preferred_element_type=F32)
-    up_delta = (act_grad * gate * sigma).astype(BF16)
-    gate_delta = (act_grad * upper * sigma * (1.0 + gate * (1.0 - sigma))).astype(BF16)
-    slot_part = lax.dot_general(gate_delta, w_gate, (NT, ((), ())), preferred_element_type=F32)
-    slot_part = slot_part + lax.dot_general(
-        up_delta, w_upper, (NT, ((), ())), preferred_element_type=F32
-    )
-    summed = lax.psum_scatter(slot_part.astype(BF16), "tp", scatter_dimension=1, tiled=True)
-    grad_gate = lax.dot_general(inputs, gate_delta, (TN, ((), ())), preferred_element_type=F32)
-    grad_up = lax.dot_general(inputs, up_delta, (TN, ((), ())), preferred_element_type=F32)
-    backrows = lax.all_to_all(
-        summed.reshape(devices, capacity, quarter), SP, split_axis=0, concat_axis=0, tiled=True
-    ).reshape(slots, quarter)
-    moe_grad = lax.dot_general(chosen, backrows, (TN, ((), ())), preferred_element_type=F32)
-    stream_part = (own_columns.astype(F32) + moe_grad).astype(BF16)
-    stream_grad = lax.all_gather(stream_part, "tp", axis=1, tiled=True)
+    stream_grad, grad_gate, grad_up, grad_down, o, mixed_rows, entry = experts(
+        chosen,
+        weight,
+        layer_grad,
+        slot_tokens,
+        gate_proj,
+        up_proj,
+        down_proj,
+        queries,
+        keys,
+        values,
+        fwd_decay,
+        bwd_decay,
+    )
     terms = lax.dot_general(
         stream_grad, mixed_rows, (TN, ((), ())), preferred_element_type=F32
     ).astype(BF16)
@@ -515,9 +810,9 @@
         stream_grad, out_proj, queries, keys, values, fwd_decay, bwd_decay, o, entry
     )
     return (
-        grad_gate.astype(BF16)[None],
-        grad_up.astype(BF16)[None],
-        grad_down.astype(BF16)[None],
+        grad_gate[None],
+        grad_up[None],
+        grad_down[None],
         proj_grad,
         query_grad,
         key_grad,

time: 256 us -> 158 us (0.62)
  Pallas kernels: 64.2 us -> 136 us
  waiting for transfers between devices: 55.5 us -> 0.01 us
  blocking collectives: 52.1 us -> 0 us
  matrix products: 20.6 us -> 2.93 us
  starting transfers between devices: 24.1 us -> 8.12 us
  between operations: 14.3 us -> 0.74 us
  local copies, waits for them, and re-layouts: 20.8 us -> 7.83 us
    pallas_call x1, Pallas kernels: 37.7 us -> 98.1 us  [experts(): pl.pallas_call(expert_kernel, out_shape=(jax.ShapeDtypeStruct((tokens, wi...]
    all_to_all x1 -> x0, blocking collectives: 41.2 us -> none  [on_device(): lax.all_to_all(outgoing.reshape(devices, capacity, quarter), SP, split_ax...]
    reduce_scatter x1 -> x0, waiting for transfers between devices: 30.6 us -> none  [on_device(): lax.psum_scatter(slot_part.astype(BF16), 'tp', scatter_dimension=1, tiled...]
    all_to_all x2 -> x0, waiting for transfers between devices: 24.9 us -> none  [the longest x1 24.9 us: copy_for_each(): lax.all_to_all(jnp.broadcast_to(array[None], (devices, *array.shape)), ax...]
    dot_general x10 -> x0, matrix products: 18.8 us -> none  [the longest x1 4.04 us: on_device(): lax.dot_general(act, inbound, (TN, ((), ())), preferred_element_type=F32)]
    all_to_all x2 -> x0, starting transfers between devices: 15.4 us -> none  [the longest x1 10.7 us: on_device(): lax.all_to_all(summed.reshape(devices, capacity, quarter), SP, split_axis...]
    pallas_call x1, Pallas kernels: 26.6 us -> 37.5 us  [attention_backward(): pl.pallas_call(backward_kernel, out_shape=(jax.ShapeDtypeStruct((tokens,...]
    all_gather x1 -> x0, blocking collectives: 10.9 us -> none  [on_device(): stream_grad = lax.all_gather(stream_part, 'tp', axis=1, tiled=True)]
  transfers between devices with their start and end apart: 4 -> 1, of which waited for: 2 -> 0; matrix products, arithmetic and copies ran while one was open for 5% -> 0% of each run, Pallas kernels for 25% -> 24%
where the time goes in v2:
time: 158 us
  Pallas kernels  136 us (86%)
  starting transfers between devices  8.12 us (5%)
  local copies, waits for them, and re-layouts  7.83 us (5%)
  matrix products  2.93 us (2%)
  other arithmetic  2.67 us (2%)
    pallas_call x1, Pallas kernels, experts(): pl.pallas_call(expert_kernel, out_shape=(jax.ShapeDtypeStruct((tokens, wi...  98.1 us
    pallas_call x1, Pallas kernels, attention_backward(): pl.pallas_call(backward_kernel, out_shape=(jax.ShapeDtypeStruct((tokens,...  37.5 us
    all_to_all x1, starting transfers between devices, on_device(): lax.all_to_all(terms.reshape(devices, -1, terms.shape[1]), SP, split_axis...  8.12 us
    unnamed x19, local copies, waits for them, and re-layouts  5.61 us
  transfers between devices with their start and end apart: 1, of which 0 were waited for; matrix products, arithmetic and copies ran while one was open for 0% of the time, Pallas kernels for 24%

profile of v2, /device:TPU:1, one launch (start us, length us, event | category | flops | bytes accessed | tf_op | source)
XLA Modules:
  0.0 157.9 jit_solution(8272996423171090819)
XLA Ops:
  0.7 0.7 broadcast_multiply_fusion
  1.4 0.8 copy.24
  2.1 0.8 fusion.27
  2.9 0.1 copy.26
  3.0 0.1 eq.49
  3.2 0.3 fusion
  3.5 0.1 convert_element_type.25
  3.7 0.2 slice_reduce_fusion.1
  3.9 0.9 fusion.3.chosen
  4.8 0.3 fusion.2
  5.0 0.9 broadcast_in_dim.59.weight
  5.9 98.1 %experts.1 = (bf16[192,2048]{1,0:T(8,128)(2,1)}, bf16[2048,256]{1,0:T(8,128)(2,1)}, bf16[2048,256]{1,0:T(8,128)(2,1)}, bf16[256,2048]{1,0:T(8,128)(2,1)}, f32[3,...) custom-call(bf16[576,192]{1,0:T(8,128)(2,1)} %fusion.3.chosen, ...), custom_call_target="tpu_custom_call" | custom-call | flops 6000000000 | bytes 10485760 | tf_op jit(solution)/shard_map/experts/pallas_call | solution.py:682
  104.0 2.6 %convolution_convert_fusion = bf16[2048,256]{1,0:T(8,128)(2,1)} fusion(bf16[192,2048]{1,0:T(8,128)(2,1)} %get-tuple-element.20.stream, bf16[192,256]{1,0:T(8,128)(2,1)} %get-tuple-element.21), kind=kOutput, calls=%fused_computation | convolution fusion | flops 201850880 | bytes 1933312 | tf_op jit(solution)/shard_map/dot_general | solution.py:802
  106.6 8.1 %all-to-all-start = ((bf16[64,32,256]{2,1,0:T(8,128)(2,1)}), bf16[64,32,256]{2,1,0:T(8,128)(2,1)S(1)}, u32[]{:S(2)}, u32[]{:S(2)}) async-start(bf16[64,32,256]{2,1,0:T(8,128)(2,1)} %bitcast.5), calls=%async_computation | async-start | bytes 2097152 | tf_op jit(solution)/shard_map/all_to_all | solution.py:805
  114.8 0.0 copy-start.2
  114.8 37.5 %attention_backward.1 = (bf16[192,128]{1,0:T(8,128)(2,1)}, bf16[192,128]{1,0:T(8,128)(2,1)}, bf16[192,256]{1,0:T(8,128)(2,1)}) custom-call(bf16[192,2048]{1,0:T(8,128)(2,1)} %get-tuple-element.20.stream, bf16[2048,256]{1,0:T(8,128)(2,1)} %out_proj.1, bf16[192,128]{1,0:T(8,128)(2,1)} %q.3, bf16[192,128]{1,0:T(8,128)(2,1)} %k.3, bf16[192,256]{1,0:T(8,128)(2,1)} %v.3, ...), custom_call_target="tpu_custom_call" | custom-call | flops 1000000000 | bytes 2097152 | tf_op jit(solution)/shard_map/attention_backward/pallas_call | solution.py:729
  152.3 0.0 all-to-all-done
  152.3 0.8 convert_reduce_fusion
  153.1 1.0 copy.34
  154.1 1.0 copy.35
  155.1 1.0 copy.36
  156.1 0.6 copy.37
  156.7 0.6 copy.38
  157.3 0.6 copy.39
  (15 shorter events, 0.1 us)
Async XLA Ops:
  106.6 45.7 %all-to-all-start = ((bf16[64,32,256]{2,1,0:T(8,128)(2,1)}), bf16[64,32,256]{2,1,0:T(8,128)(2,1)S(1)}, u32[]{:S(2)}, u32[]{:S(2)}) async-start(bf16[64,32,256]{2,1,0:T(8,128)(2,1)} %bitcast.5), calls=%async_computation | async-start | bytes 2097152 | tf_op jit(solution)/shard_map/all_to_all | solution.py:805
  114.8 38.4 %copy-start.2 = (bf16[2048,256]{1,0:T(8,128)(2,1)S(1)}, bf16[2048,256]{1,0:T(8,128)(2,1)}, u32[]{:S(2)}) copy-start(bf16[2048,256]{1,0:T(8,128)(2,1)} %get-tuple-element.17) | copy-start | bytes 3145732
  152.3 1.8 %copy-start.1 = (bf16[2048,256]{1,0:T(8,128)(2,1)S(1)}, bf16[2048,256]{1,0:T(8,128)(2,1)}, u32[]{:S(2)}) copy-start(bf16[2048,256]{1,0:T(8,128)(2,1)} %get-tuple-element.18) | copy-start | bytes 3145732
  153.1 2.0 %copy-start = (bf16[256,2048]{1,0:T(8,128)(2,1)S(1)}, bf16[256,2048]{1,0:T(8,128)(2,1)}, u32[]{:S(2)}) copy-start(bf16[256,2048]{1,0:T(8,128)(2,1)} %get-tuple-element.19) | copy-start | bytes 3145732
  154.1 2.0 %copy-start.5 = (bf16[192,128]{1,0:T(8,128)(2,1)S(1)}, bf16[192,128]{1,0:T(8,128)(2,1)}, u32[]{:S(2)}) copy-start(bf16[192,128]{1,0:T(8,128)(2,1)} %get-tuple-element.42) | copy-start | bytes 147460
  154.1 2.6 %copy-start.4 = (bf16[192,128]{1,0:T(8,128)(2,1)S(1)}, bf16[192,128]{1,0:T(8,128)(2,1)}, u32[]{:S(2)}) copy-start(bf16[192,128]{1,0:T(8,128)(2,1)} %get-tuple-element.43) | copy-start | bytes 147460
  154.1 3.2 %copy-start.3 = (bf16[192,256]{1,0:T(8,128)(2,1)S(1)}, bf16[192,256]{1,0:T(8,128)(2,1)}, u32[]{:S(2)}) copy-start(bf16[192,256]{1,0:T(8,128)(2,1)} %get-tuple-element.44) | copy-start | bytes 294916

commit v3 on v2

--- a/solution.py
+++ b/solution.py
@@ -301,30 +301,33 @@
     return jnp.where(source == iota(shape, 1), 1.0, 0.0).astype(BF16)
 
 
-def expert_kernel(
-    chosen,
-    weight,
+def layer_kernel(
+    routes,
+    route_weight,
     layer_grad,
     slot_tokens,
     gate_proj,
     up_proj,
     down_proj,
+    out_proj,
     q,
     k,
     v,
     fd,
     bd,
-    stream_ref,
     gate_grad_ref,
     up_grad_ref,
     down_grad_ref,
-    o_ref,
-    rows_ref,
-    entry_ref,
+    proj_ref,
+    dq_ref,
+    dk_ref,
+    dv_ref,
     own,
     x,
     w_cat,
     w_down,
+    w_out,
+    choice,
     swap,
     act,
     silu,
@@ -344,12 +347,18 @@
     back_out,
     back_in,
     stream,
+    terms,
+    core_in,
+    core_sum,
+    row_in,
+    row_sum,
+    depth_in,
     send,
     recv,
     load,
     *carry_refs,
 ):
-    z, _, _, p = position()
+    z, y, c, p = position()
     t = lax.axis_index("tp")
     right, left, across = lax.rem(t + 1, RING), lax.rem(t + 3, RING), lax.rem(t + 2, RING)
     quarter = own.shape[1]
@@ -365,6 +374,7 @@
         pltpu.make_async_copy(gate_proj.at[0], w_cat.at[:, pl.ds(0, hidden)], load.at[2]),
         pltpu.make_async_copy(up_proj.at[0], w_cat.at[:, pl.ds(hidden, hidden)], load.at[3]),
         pltpu.make_async_copy(down_proj.at[0], w_down, load.at[4]),
+        pltpu.make_async_copy(out_proj, w_out, load.at[5]),
     ]
     for copy in loads:
         copy.start()
@@ -380,8 +390,28 @@
         other, device = plane_peer(p, PLANES - d, PLANES)
         return remote(out.at[other], into.at[other], sems(kind, d), device)
 
+    tokens = own.shape[0]
+    slots = x.shape[0]
+    lanes = iota((tokens, 128), 1)
+    first = (routes[:, 0:1] == lanes).astype(BF16)
+    second = (routes[:, 1:2] == lanes).astype(BF16)
+    shape = (tokens, tokens)
+    earlier = (iota(shape, 0) > iota(shape, 1)).astype(BF16)
+    before = dot(earlier, first + second)
     loads[0].wait()
-    picked = dot(chosen[...], own[...]) * weight[...]
+    mine = own[...].astype(F32)
+    weighted = []
+    for j, members in enumerate((first, second)):
+        named = members.astype(F32)
+        rank = jnp.sum((before + first.astype(F32) * j) * named, axis=1, keepdims=True)
+        rank = rank.astype(jnp.int32)
+        expert = routes[:, j : j + 1]
+        row = (expert & (PLANES - 1)) * CHUNK + (expert >> 3) * CAP + rank
+        row = jnp.where(rank < CAP, row, -1)
+        taken = (row == iota((tokens, slots), 1)).astype(BF16)
+        choice[j * tokens : (j + 1) * tokens, :] = taken
+        weighted.append((mine * route_weight[:, j : j + 1]).astype(BF16))
+    picked = dot(choice[...], jnp.concatenate(weighted, axis=0), TN)
     out_plane[...] = picked.astype(BF16).reshape(out_plane.shape)
     pl.semaphore_wait(barrier, count + 2)
     for d in PLANE_ORDER:
@@ -395,39 +425,9 @@
     _, _, forward_end, backward_end = both_states(pieces, zero, zero)
     log_f = sum(piece.last for piece in pieces)
     log_b = sum(piece.first for piece in pieces)
-    carry = Carry(carry_refs)
+    carry = Carry(carry_refs[:12])
     carry.start((forward_end, backward_end), (log_f, log_b))
     swap[...] = swap_matrix(swap.shape)
-
-    for d in PLANE_ORDER:
-        plane_in(0, out_plane, in_plane, d).wait_recv()
-    moved = dot(swap[...], in_plane[...].reshape(DEPTH * CHUNK, quarter)).astype(BF16)
-    out_depth[...] = moved.reshape(out_depth.shape)
-    carry.middle()
-
-    def depth_out(i):
-        other = lax.rem(z + DEPTH - OFFSETS[i], DEPTH)
-        return remote(out_depth.at[other], inbound.at[t, z], sems(1, i), {"sp_0": other})
-
-    for i in range(1, DEPTH):
-        depth_out(i).start()
-    inbound[t, z] = out_depth[z]
-
-    for copy in loads[1:4]:
-        copy.wait()
-    half = x.shape[0] // 2
-    for j in range(2):
-        rows = pl.ds(j * half, half)
-        chunks = pl.ds(j * (DEPTH // 2), DEPTH // 2)
-        both_up = jnp.dot(x[rows, :], w_cat[...], preferred_element_type=F32)
-        gate, up = both_up[:, :hidden], both_up[:, hidden:]
-        sigma = jax.nn.sigmoid(gate)
-        s = gate * sigma
-        shape = (DEPTH // 2, CHUNK, hidden)
-        silu[chunks] = s.reshape(shape)
-        act[chunks] = (s * up).astype(BF16).reshape(shape)
-        slope[chunks] = (up * sigma * (1.0 + gate * (1.0 - sigma))).reshape(shape)
-    loads[4].wait()
 
     def chunk_of(i):
         return lax.rem(z + OFFSETS[i], DEPTH)
@@ -513,32 +513,60 @@
             ret_out[at] = total.astype(BF16)
             send_back(i).start()
 
+    for d in PLANE_ORDER:
+        plane_in(0, out_plane, in_plane, d).wait_recv()
+    moved = dot(swap[...], in_plane[...].reshape(DEPTH * CHUNK, quarter)).astype(BF16)
+    out_depth[...] = moved.reshape(out_depth.shape)
+
+    def depth_out(i):
+        other = lax.rem(z + DEPTH - OFFSETS[i], DEPTH)
+        return remote(out_depth.at[other], inbound.at[t, z], sems(1, i), {"sp_0": other})
+
+    inbound[t, z] = out_depth[z]
+    stage_0(0)
+    for i in range(1, DEPTH):
+        depth_out(i).start()
+    carry.middle()
+
+    for copy in loads[1:4]:
+        copy.wait()
+    half = x.shape[0] // 2
+    for j in range(2):
+        rows = pl.ds(j * half, half)
+        chunks = pl.ds(j * (DEPTH // 2), DEPTH // 2)
+        both_up = jnp.dot(x[rows, :], w_cat[...], preferred_element_type=F32)
+        gate, up = both_up[:, :hidden], both_up[:, hidden:]
+        sigma = jax.nn.sigmoid(gate)
+        s = gate * sigma
+        shape = (DEPTH // 2, CHUNK, hidden)
+        silu[chunks] = s.reshape(shape)
+        act[chunks] = (s * up).astype(BF16).reshape(shape)
+        slope[chunks] = (up * sigma * (1.0 + gate * (1.0 - sigma))).reshape(shape)
+    loads[4].wait()
+
     stages = (stage_0, stage_1, stage_2, stage_3, stage_4)
     for n in range(DEPTH + len(stages) - 1):
         for lag, stage in enumerate(stages):
-            if 0 <= n - lag < DEPTH:
+            if 0 <= n - lag < DEPTH and (n > 0 or lag > 0):
                 stage(n - lag)
-        if n == 0:
+        if n == 2:
+            inclusive, strict = masks()
+            for piece in pieces:
+                piece.a = piece.scores(inclusive, strict)
+                piece.inner = dot(piece.a, piece.vs)
+                piece.entries()
+        if n == 5:
             carry.last()
-        if n == 1:
-            inclusive, strict = masks()
-            inner = []
-            for piece in pieces:
-                inner.append(dot(piece.scores(inclusive, strict), piece.vs))
-                piece.entries()
-        if n == 3:
+        if n == 8:
             forward_entry, backward_entry = carry.finish()
-            entry_ref[0] = forward_entry
-            entry_ref[1] = backward_entry
             before, after, _, _ = both_states(pieces, forward_entry, backward_entry)
             for b, piece in enumerate(pieces):
-                across_state = jnp.concatenate([before[b], after[b]], axis=1)
-                o = inner[b] + dot(
-                    jnp.concatenate([piece.qg, piece.qh], axis=1), across_state, NT
+                piece.states = jnp.concatenate([before[b], after[b]], axis=1).astype(BF16)
+                o = piece.inner + dot(
+                    jnp.concatenate([piece.qg, piece.qh], axis=1), piece.states, NT
                 )
-                o_ref[b] = o
-                mixed = o * lax.rsqrt(jnp.mean(o * o, axis=1, keepdims=True) + EPSILON)
-                rows_ref[pl.ds(b * BLOCK, BLOCK), :] = heads_on_lanes(mixed).astype(BF16)
+                piece.inv = lax.rsqrt(jnp.mean(o * o, axis=1, keepdims=True) + EPSILON)
+                piece.mixed = o * piece.inv
 
     act_all = act[...].reshape(DEPTH * CHUNK, hidden)
     for n in range(RING):
@@ -560,35 +588,153 @@
         up_grad_ref[rows, :] = both_grads[:, hidden:].astype(BF16)
     for d in PLANE_ORDER:
         plane_in(9, back_out, back_in, d).wait_recv()
-    moe_grad = dot(chosen[...], back_in[...].reshape(DEPTH * CHUNK, quarter), TN)
+    taken = choice[:tokens, :] + choice[tokens:, :]
+    moe_grad = dot(taken, back_in[...].reshape(DEPTH * CHUNK, quarter))
     stream[t] = (own[...].astype(F32) + moe_grad).astype(BF16)
 
-    tokens = own.shape[0]
-
-    def stream_spread(arriving=False):
-        a, b = (left, right) if arriving else (t, t)
+    low, high = pl.ds(0, tokens // 2), pl.ds(tokens // 2, tokens // 2)
+
+    def ring(kind, which, rows, to):
+        return remote(stream.at[which, rows], stream.at[which, rows], sems(kind, 0), {"tp": to})
+
+    def stream_spread():
         return (
-            remote(stream.at[a], stream.at[a], sems(0, 0), {"tp": right}),
-            remote(stream.at[b], stream.at[b], sems(1, 0), {"tp": left}),
+            ring(0, t, low, right),
+            ring(1, t, high, left),
+            ring(2 + 6, t, high, right),
+            ring(3 + 6, t, low, left),
         )
 
-    def stream_pass(arriving=False):
-        top, low = pl.ds(0, tokens // 2), pl.ds(tokens // 2, tokens // 2)
-        a, b = (across, across) if arriving else (left, right)
+    def stream_arrived():
         return (
-            remote(stream.at[a, top], stream.at[a, top], sems(8, 0), {"tp": right}),
-            remote(stream.at[b, low], stream.at[b, low], sems(9, 0), {"tp": left}),
+            ring(0, left, low, right),
+            ring(1, right, high, left),
+            ring(2 + 6, left, high, right),
+            ring(3 + 6, right, low, left),
+        )
+
+    def stream_pass(which_low, which_high):
+        return (
+            remote(
+                stream.at[which_low, low], stream.at[which_low, low], sems(10, 0), {"tp": right}
+            ),
+            remote(
+                stream.at[which_high, high], stream.at[which_high, high], sems(11, 0), {"tp": left}
+            ),
         )
 
     for copy in stream_spread():
         copy.start()
-    for copy, onward in zip(stream_spread(True), stream_pass()):
+    loads[5].wait()
+
+    def share(which):
+        rows = pl.ds(pl.multiple_of(which * quarter, quarter), quarter)
+        return jnp.dot(stream[which], w_out[rows, :], preferred_element_type=F32)
+
+    mixed_grad = share(t)
+    for n, copy in enumerate(stream_arrived()):
         copy.wait_recv()
-        onward.start()
-    for copy in stream_pass(True):
+        if n < 2:
+            stream_pass(left, right)[n].start()
+    mixed_grad = mixed_grad + share(left) + share(right)
+    for copy in stream_pass(across, across):
         copy.wait_recv()
+    mixed_grad = mixed_grad + share(across)
+
+    back_c, back_d = jnp.zeros((DV, 128), F32), jnp.zeros((DV, 128), F32)
+    for b, piece in enumerate(pieces):
+        mg = heads_on_rows(mixed_grad[b * BLOCK : (b + 1) * BLOCK, :])
+        mean = jnp.mean(mg * piece.mixed, axis=1, keepdims=True)
+        piece.do = (piece.inv * (mg - piece.mixed * mean)).astype(BF16)
+        piece.back_f = dot(piece.do, piece.qg, TN)
+        piece.back_b = dot(piece.do, piece.qh, TN)
+    for piece in pieces:
+        back_c = back_c * jnp.exp(piece.first) + piece.back_b
+    for piece in reversed(pieces):
+        back_d = back_d * jnp.exp(piece.last) + piece.back_f
+    carry = Carry(carry_refs[12:])
+    carry.start((back_c, back_d), (log_b, log_f))
+
+    rows_of_mixed = jnp.concatenate([heads_on_lanes(piece.mixed) for piece in pieces], axis=0)
+    rows_of_mixed = rows_of_mixed.astype(BF16)
+    piece_rows = proj_ref.shape[0]
     for n in range(RING):
-        stream_ref[:, n * quarter : (n + 1) * quarter] = stream[n]
+        term = dot(stream[n], rows_of_mixed, TN).astype(BF16)
+        per = term.shape[0] // (piece_rows * PLANES)
+        term = term.reshape(per, 4, 2, piece_rows, term.shape[1])
+        for cc in range(2):
+            for zz in range(per):
+                terms[cc, :, n * per + zz] = term[zz, :, cc]
+
+    def core_copy():
+        return remote(terms.at[1 - c], core_in, sems(12, 0), {"sp_2": 1 - c})
+
+    def row_copy(d, arriving=False):
+        other = lax.rem(y + (4 - d if arriving else d), 4)
+        at = other if arriving else y
+        return remote(core_sum.at[other], row_in.at[at], sems(12, d), {"sp_1": other})
+
+    def last_copy(d, arriving=False):
+        other = lax.rem(z + (DEPTH - d if arriving else d), DEPTH)
+        at = other if arriving else z
+        return remote(row_sum.at[other], depth_in.at[at], sems(13, d), {"sp_0": other})
+
+    core_copy().start()
+
+    inclusive, strict = masks()
+    for piece in pieces:
+        da = dot(piece.do, piece.vs, NT)
+        da_f = jnp.where(inclusive, da, 0.0).astype(BF16)
+        da_b = jnp.where(strict, da, 0.0).astype(BF16)
+        piece.dv = dot(piece.a, piece.do, TN)
+        piece.dq = dot(da_f, piece.k_dn_g) * doubled(piece.up_g) + dot(
+            da_b, piece.k_dn_h
+        ) * doubled(piece.up_h)
+        piece.dk = dot(da_f, piece.q_up_g, TN) * doubled(piece.dn_g) + dot(
+            da_b, piece.q_up_h, TN
+        ) * doubled(piece.dn_h)
+    carry.middle()
+    core_copy().wait_recv()
+    core_sum[...] = (terms[c].astype(F32) + core_in[...].astype(F32)).astype(BF16)
+    for d in (2, 1, 3):
+        row_copy(d).start()
+    for b, piece in enumerate(pieces):
+        dq = dot(piece.do, piece.states)
+        dq = piece.dq + dq[:, :128] * stacked(piece.eg) + dq[:, 128:] * stacked(piece.eh)
+        dq_ref[pl.ds(b * BLOCK, BLOCK), :] = (folded(dq) * KEY_CHANNELS**-0.5).astype(BF16)
+    carry.last()
+    for d in (1, 3, 2):
+        row_copy(d, True).wait_recv()
+    row_in[y] = core_sum[y]
+    total = row_in[0].astype(F32)
+    for n in range(1, 4):
+        total = total + row_in[n].astype(F32)
+    row_sum[...] = total
+    for d in (4, 3, 5, 2, 6, 1, 7):
+        last_copy(d).start()
+    back_c, back_d = carry.finish()
+    late, early = [None] * 3, [None] * 3
+    for b, piece in enumerate(pieces):
+        early[b] = back_c
+        back_c = back_c * jnp.exp(piece.first) + piece.back_b
+    for b in reversed(range(3)):
+        late[b] = back_d
+        back_d = back_d * jnp.exp(pieces[b].last) + pieces[b].back_f
+    for b, piece in enumerate(pieces):
+        states = jnp.concatenate([late[b], early[b]], axis=1).astype(BF16)
+        dk = dot(piece.vs, states)
+        dk = piece.dk + dk[:, :128] * stacked(piece.eg_end) + dk[:, 128:] * stacked(piece.eh_end)
+        dv = piece.dv + dot(jnp.concatenate([piece.kg_end, piece.kh_end], axis=1), states, NT)
+        rows = pl.ds(b * BLOCK, BLOCK)
+        dk_ref[rows, :] = folded(dk).astype(BF16)
+        dv_ref[rows, :] = heads_on_lanes(dv).astype(BF16)
+    depth_in[z] = row_sum[z]
+    for d in range(1, DEPTH):
+        last_copy(d, True).wait_recv()
+    total = depth_in[0]
+    for n in range(1, DEPTH):
+        total = total + depth_in[n]
+    proj_ref[...] = total
 
     for d in PLANE_ORDER:
         plane_out(0, out_plane, in_plane, d).wait_send()
@@ -599,104 +745,48 @@
             send_back(i).wait_send()
         for copy in (*spread(i), pass_on(i), send_hop(i), send_both(i), send_plain(i)):
             copy.wait_send()
-    for copy in (*stream_spread(), *stream_pass()):
+    for copy in (*stream_spread(), *stream_pass(left, right), core_copy()):
         copy.wait_send()
-
-
-def backward_kernel(
-    stream, out_proj, q, k, v, fd, bd, o_ref, entry_ref, dq_ref, dk_ref, dv_ref, *scratch
-):
-    barrier, count = greet(8, 8)
-    pieces = [Piece(b, q, k, v, fd, bd) for b in range(3)]
-    mixed_grad = jnp.dot(stream[...], out_proj[...], preferred_element_type=F32)
-    c, d = jnp.zeros((DV, 128), F32), jnp.zeros((DV, 128), F32)
-    for b, piece in enumerate(pieces):
-        o = o_ref[b]
-        inv = lax.rsqrt(jnp.mean(o * o, axis=1, keepdims=True) + EPSILON)
-        mixed = o * inv
-        mg = heads_on_rows(mixed_grad[b * BLOCK : (b + 1) * BLOCK, :])
-        piece.do = (inv * (mg - mixed * jnp.mean(mg * mixed, axis=1, keepdims=True))).astype(BF16)
-        piece.entries()
-        piece.back_f = dot(piece.do, piece.qg, TN)
-        piece.back_b = dot(piece.do, piece.qh, TN)
-    for piece in pieces:
-        c = c * jnp.exp(piece.first) + piece.back_b
-    for piece in reversed(pieces):
-        d = d * jnp.exp(piece.last) + piece.back_f
-    log_f = sum(piece.last for piece in pieces)
-    log_b = sum(piece.first for piece in pieces)
-    pl.semaphore_wait(barrier, count)
-    carry = Carry(scratch)
-    carry.start((c, d), (log_b, log_f))
-    inclusive, strict = masks()
-    for piece in pieces:
-        a = piece.scores(inclusive, strict)
-        da = dot(piece.do, piece.vs, NT)
-        da_f = jnp.where(inclusive, da, 0.0).astype(BF16)
-        da_b = jnp.where(strict, da, 0.0).astype(BF16)
-        piece.dv = dot(a, piece.do, TN)
-        piece.dq = dot(da_f, piece.k_dn_g) * doubled(piece.up_g) + dot(
-            da_b, piece.k_dn_h
-        ) * doubled(piece.up_h)
-        piece.dk = dot(da_f, piece.q_up_g, TN) * doubled(piece.dn_g) + dot(
-            da_b, piece.q_up_h, TN
-        ) * doubled(piece.dn_h)
-    carry.middle()
-    for piece in pieces:
-        piece.ends()
-    before, after, _, _ = both_states(pieces, entry_ref[0], entry_ref[1])
-    for b, piece in enumerate(pieces):
-        dq = dot(piece.do, jnp.concatenate([before[b], after[b]], axis=1))
-        piece.dq = piece.dq + dq[:, :128] * stacked(piece.eg) + dq[:, 128:] * stacked(piece.eh)
-        dq_ref[pl.ds(b * BLOCK, BLOCK), :] = (folded(piece.dq) * KEY_CHANNELS**-0.5).astype(BF16)
-    carry.last()
-    c, d = carry.finish()
-    late, early = [None] * 3, [None] * 3
-    for b, piece in enumerate(pieces):
-        early[b] = c
-        c = c * jnp.exp(piece.first) + piece.back_b
-    for b in reversed(range(3)):
-        late[b] = d
-        d = d * jnp.exp(pieces[b].last) + pieces[b].back_f
-    for b, piece in enumerate(pieces):
-        states = jnp.concatenate([late[b], early[b]], axis=1).astype(BF16)
-        dk = dot(piece.vs, states)
-        dk = piece.dk + dk[:, :128] * stacked(piece.eg_end) + dk[:, 128:] * stacked(piece.eh_end)
-        dv = piece.dv + dot(jnp.concatenate([piece.kg_end, piece.kh_end], axis=1), states, NT)
-        rows = pl.ds(b * BLOCK, BLOCK)
-        dk_ref[rows, :] = folded(dk).astype(BF16)
-        dv_ref[rows, :] = heads_on_lanes(dv).astype(BF16)
+    for d in (1, 2, 3):
+        row_copy(d).wait_send()
+    for d in range(1, DEPTH):
+        last_copy(d).wait_send()
 
 
 def vmem(n):
     return [pl.BlockSpec(memory_space=pltpu.VMEM)] * n
 
 
-def experts(chosen, weight, layer_grad, slot_tokens, gate, up, down, q, k, v, fd, bd):
+def layer(*arrays):
+    layer_grad, slot_tokens, gate = arrays[2], arrays[3], arrays[4]
     tokens, width = layer_grad.shape
     slots = slot_tokens.shape[1]
     quarter = width // RING
     hidden = gate.shape[2]
+    out_columns = arrays[7].shape[1]
+    piece_rows = width // (DEPTH * PLANES)
     rows = (DEPTH, CHUNK, quarter)
     anywhere = pl.BlockSpec(memory_space=pl.ANY)
     return pl.pallas_call(
-        expert_kernel,
+        layer_kernel,
         out_shape=(
-            jax.ShapeDtypeStruct((tokens, width), BF16),
             jax.ShapeDtypeStruct((width, hidden), BF16),
             jax.ShapeDtypeStruct((width, hidden), BF16),
             jax.ShapeDtypeStruct((hidden, width), BF16),
-            jax.ShapeDtypeStruct((3, 128, DV), F32),
+            jax.ShapeDtypeStruct((piece_rows, out_columns), F32),
+            jax.ShapeDtypeStruct((tokens, 128), BF16),
+            jax.ShapeDtypeStruct((tokens, 128), BF16),
             jax.ShapeDtypeStruct((tokens, 2 * DV), BF16),
-            jax.ShapeDtypeStruct((2, DV, 128), F32),
         ),
-        in_specs=vmem(2) + [anywhere] * 5 + vmem(5),
+        in_specs=vmem(2) + [anywhere] * 6 + vmem(5),
         out_specs=tuple(vmem(7)),
         scratch_shapes=[
             pltpu.VMEM((tokens, quarter), BF16),
             pltpu.VMEM((slots, width), BF16),
             pltpu.VMEM((width, 2 * hidden), BF16),
             pltpu.VMEM((hidden, width), BF16),
+            pltpu.VMEM((width, out_columns), BF16),
+            pltpu.VMEM((2 * tokens, slots), BF16),
             pltpu.VMEM((slots, slots), BF16),
             pltpu.VMEM((DEPTH, CHUNK, hidden), BF16),
             pltpu.VMEM((DEPTH, CHUNK, hidden), F32),
@@ -709,115 +799,31 @@
             pltpu.VMEM((DEPTH, RING, CHUNK, quarter), BF16),
             *[pltpu.VMEM(rows, BF16)] * 8,
             pltpu.VMEM((RING, tokens, quarter), BF16),
-            pltpu.SemaphoreType.DMA((10, DEPTH)),
-            pltpu.SemaphoreType.DMA((10, DEPTH)),
-            pltpu.SemaphoreType.DMA((5,)),
+            pltpu.VMEM((2, 4, DEPTH, piece_rows, out_columns), BF16),
+            pltpu.VMEM((4, DEPTH, piece_rows, out_columns), BF16),
+            pltpu.VMEM((4, DEPTH, piece_rows, out_columns), BF16),
+            pltpu.VMEM((4, DEPTH, piece_rows, out_columns), BF16),
+            pltpu.VMEM((DEPTH, piece_rows, out_columns), F32),
+            pltpu.VMEM((DEPTH, piece_rows, out_columns), F32),
+            pltpu.SemaphoreType.DMA((14, DEPTH)),
+            pltpu.SemaphoreType.DMA((14, DEPTH)),
+            pltpu.SemaphoreType.DMA((6,)),
+            *Carry.scratch(),
             *Carry.scratch(),
         ],
         compiler_params=pltpu.CompilerParams(
             collective_id=0, has_side_effects=True, vmem_limit_bytes=60 * 2**20
         ),
         cost_estimate=pl.CostEstimate(
-            flops=6 * 10**9, bytes_accessed=10 * 2**20, transcendentals=0
+            flops=8 * 10**9, bytes_accessed=12 * 2**20, transcendentals=0
         ),
-        name="experts",
-    )(chosen, weight, layer_grad, slot_tokens, gate, up, down, q, k, v, fd, bd)
-
-
-def attention_backward(stream, out_proj, q, k, v, fd, bd, o, entry):
-    tokens = q.shape[0]
-    return pl.pallas_call(
-        backward_kernel,
-        out_shape=(
-            jax.ShapeDtypeStruct((tokens, 128), BF16),
-            jax.ShapeDtypeStruct((tokens, 128), BF16),
-            jax.ShapeDtypeStruct((tokens, 2 * DV), BF16),
-        ),
-        in_specs=vmem(9),
-        out_specs=tuple(vmem(3)),
-        scratch_shapes=Carry.scratch(),
-        compiler_params=pltpu.CompilerParams(collective_id=1, has_side_effects=True),
-        cost_estimate=pl.CostEstimate(
-            flops=10**9, bytes_accessed=2**21, transcendentals=0
-        ),
-        name="attention_backward",
-    )(stream, out_proj, q, k, v, fd, bd, o, entry)
-
-
-def slot_choice(routes, weights, experts, slots):
-    tokens = routes.shape[0]
-    ids = routes.reshape(-1)
-    members = (ids[:, None] == jnp.arange(experts, dtype=jnp.int32)[None, :]).astype(BF16)
-    earlier = jnp.tril(jnp.ones((2 * tokens, 2 * tokens), BF16), -1)
-    before = jnp.dot(earlier, members, preferred_element_type=F32)
-    ranks = jnp.sum(before * members.astype(F32), axis=1).astype(jnp.int32)
-    target = jnp.where(ranks < CAP, ids * CAP + ranks, -1).reshape(tokens, 2)
-    row = jnp.arange(slots, dtype=jnp.int32)
-    expert = (row // CAP) % DEPTH * PLANES + row // CHUNK
-    slot = (expert * CAP + row % CAP)[:, None]
-    first = slot == target[:, 0][None, :]
-    second = slot == target[:, 1][None, :]
-    chosen = (first | second).astype(BF16)
-    weight = jnp.sum(
-        jnp.where(first, weights[:, 0][None, :], 0.0)
-        + jnp.where(second, weights[:, 1][None, :], 0.0),
-        axis=1,
-        keepdims=True,
-    )
-    return chosen, weight
-
-
-def on_device(
-    layer_grad,
-    routes,
-    route_weight,
-    slot_tokens,
-    gate_proj,
-    up_proj,
-    down_proj,
-    out_proj,
-    queries,
-    keys,
-    values,
-    fwd_decay,
-    bwd_decay,
-):
-    devices = lax.axis_size(SP)
-    slots = slot_tokens.shape[1]
-    chosen, weight = slot_choice(routes, route_weight, devices, slots)
-    stream_grad, grad_gate, grad_up, grad_down, o, mixed_rows, entry = experts(
-        chosen,
-        weight,
-        layer_grad,
-        slot_tokens,
-        gate_proj,
-        up_proj,
-        down_proj,
-        queries,
-        keys,
-        values,
-        fwd_decay,
-        bwd_decay,
-    )
-    terms = lax.dot_general(
-        stream_grad, mixed_rows, (TN, ((), ())), preferred_element_type=F32
-    ).astype(BF16)
-    arrived_terms = lax.all_to_all(
-        terms.reshape(devices, -1, terms.shape[1]), SP, split_axis=0, concat_axis=0, tiled=True
-    )
-    proj_grad = arrived_terms.astype(F32).sum(axis=0)
-    query_grad, key_grad, value_grad = attention_backward(
-        stream_grad, out_proj, queries, keys, values, fwd_decay, bwd_decay, o, entry
-    )
-    return (
-        grad_gate[None],
-        grad_up[None],
-        grad_down[None],
-        proj_grad,
-        query_grad,
-        key_grad,
-        value_grad,
-    )
+        name="layer",
+    )(*arrays)
+
+
+def on_device(layer_grad, routes, route_weight, *arrays):
+    gate, up, down, proj, query, key, value = layer(routes, route_weight, layer_grad, *arrays)
+    return gate[None], up[None], down[None], proj, query, key, value
 
 
 def solution(mesh):

time: 158 us -> 130 us (0.82)
  Pallas kernels: 136 us -> 120 us
  starting transfers between devices: 8.12 us -> 0 us
  matrix products: 2.93 us -> 0 us
  other arithmetic: 2.67 us -> 0 us
  local copies, waits for them, and re-layouts: 7.83 us -> 9.76 us
    pallas_call x2 -> x1, Pallas kernels: 136 us -> 120 us  [layer(): pl.pallas_call(layer_kernel, out_shape=(jax.ShapeDtypeStruct((width, hidd...]
    all_to_all x1 -> x0, starting transfers between devices: 8.12 us -> none  [on_device(): lax.all_to_all(terms.reshape(devices, -1, terms.shape[1]), SP, split_axis...]
    unnamed x19 -> x21, local copies, waits for them, and re-layouts: 5.61 us -> 9.76 us
    dot_general x2 -> x0, matrix products: 2.93 us -> none  [the longest x1 2.6 us: on_device(): lax.dot_general(stream_grad, mixed_rows, (TN, ((), ())), preferred_elemen...]
  transfers between devices with their start and end apart: 1 -> 0, of which waited for: 0 -> 0; matrix products, arithmetic and copies ran while one was open for 0% -> 0% of each run, Pallas kernels for 24% -> 0%
where the time goes in v3:
time: 130 us
  Pallas kernels  120 us (92%)
  local copies, waits for them, and re-layouts  9.76 us (8%)
    pallas_call x1, Pallas kernels, layer(): pl.pallas_call(layer_kernel, out_shape=(jax.ShapeDtypeStruct((width, hidd...  120 us
    unnamed x21, local copies, waits for them, and re-layouts  9.76 us

profile of v3, /device:TPU:1, one launch (start us, length us, event | category | flops | bytes accessed | tf_op | source)
XLA Modules:
  0.0 130.2 jit_solution(840540052644462693)
XLA Ops:
  0.6 1.4 %copy.20.routes = s32[192,2]{1,0:T(8,128)} copy(s32[192,2]{0,1:T(2,128)} %param.14) | data formatting | bytes 3072 | tf_op args[1]
  2.1 1.4 %copy.21.route_weight = f32[192,2]{1,0:T(8,128)} copy(f32[192,2]{0,1:T(2,128)} %param.15) | data formatting | bytes 3072 | tf_op args[2]
  3.5 119.8 %layer.1 = (bf16[2048,256]{1,0:T(8,128)(2,1)}, bf16[2048,256]{1,0:T(8,128)(2,1)}, bf16[256,2048]{1,0:T(8,128)(2,1)}, f32[32,256]{1,0:T(8,128)}, bf16[192,128]{1,...) custom-call(s32[192,2]{1,0:T(8,128)} %copy.20.routes, f32[192,2]{1,0:T(8,128)} %copy.21.route_weight, ...), custom_call_target="tpu_custom_call" | custom-call | flops 8000000000 | bytes 12582912 | tf_op jit(solution)/shard_map/layer/pallas_call | solution.py:770
  123.3 0.0 copy-start.1
  123.3 0.0 copy-start
  123.3 2.4 %copy.29 = bf16[1,2048,256]{2,1,0:T(8,128)(2,1)} copy(bf16[1,2048,256]{2,1,0:T(8,128)(2,1)} %bitcast.5) | data formatting | bytes 2097152
  125.7 0.0 copy-done.1
  125.7 0.0 copy-start.5
  125.7 0.0 copy-start.4
  125.7 0.0 copy-start.3
  125.8 0.0 copy-start.2
  125.8 1.0 copy.30
  126.7 0.0 copy-done
  126.7 1.0 copy.31
  127.7 0.0 copy-done.5
  127.7 0.6 copy.32
  128.3 0.0 copy-done.4
  128.3 0.6 copy.33
  128.9 0.0 copy-done.3
  129.0 0.6 copy.34
  129.6 0.0 copy-done.2
  129.6 0.6 copy.35
Async XLA Ops:
  123.3 2.4 %copy-start.1 = (bf16[2048,256]{1,0:T(8,128)(2,1)S(1)}, bf16[2048,256]{1,0:T(8,128)(2,1)}, u32[]{:S(2)}) copy-start(bf16[2048,256]{1,0:T(8,128)(2,1)} %get-tuple-element.15) | copy-start | bytes 3145732
  123.3 3.4 %copy-start = (bf16[256,2048]{1,0:T(8,128)(2,1)S(1)}, bf16[256,2048]{1,0:T(8,128)(2,1)}, u32[]{:S(2)}) copy-start(bf16[256,2048]{1,0:T(8,128)(2,1)} %get-tuple-element.16) | copy-start | bytes 3145732
  125.7 2.0 %copy-start.5 = (f32[32,256]{1,0:T(8,128)S(1)}, f32[32,256]{1,0:T(8,128)}, u32[]{:S(2)}) copy-start(f32[32,256]{1,0:T(8,128)} %get-tuple-element.31) | copy-start | bytes 98308
  125.7 2.6 %copy-start.4 = (bf16[192,128]{1,0:T(8,128)(2,1)S(1)}, bf16[192,128]{1,0:T(8,128)(2,1)}, u32[]{:S(2)}) copy-start(bf16[192,128]{1,0:T(8,128)(2,1)} %get-tuple-element.32) | copy-start | bytes 147460
  125.7 3.2 %copy-start.3 = (bf16[192,128]{1,0:T(8,128)(2,1)S(1)}, bf16[192,128]{1,0:T(8,128)(2,1)}, u32[]{:S(2)}) copy-start(bf16[192,128]{1,0:T(8,128)(2,1)} %get-tuple-element.33) | copy-start | bytes 147460
  125.8 3.8 %copy-start.2 = (bf16[192,256]{1,0:T(8,128)(2,1)S(1)}, bf16[192,256]{1,0:T(8,128)(2,1)}, u32[]{:S(2)}) copy-start(bf16[192,256]{1,0:T(8,128)(2,1)} %get-tuple-element.34) | copy-start | bytes 294916

commit v4 on v3

--- a/solution.py
+++ b/solution.py
@@ -310,11 +310,11 @@
     up_proj,
     down_proj,
     out_proj,
-    q,
-    k,
-    v,
-    fd,
-    bd,
+    q_hbm,
+    k_hbm,
+    v_hbm,
+    fd_hbm,
+    bd_hbm,
     gate_grad_ref,
     up_grad_ref,
     down_grad_ref,
@@ -322,12 +322,18 @@
     dq_ref,
     dk_ref,
     dv_ref,
+    q,
+    k,
+    v,
+    fd,
+    bd,
     own,
     x,
     w_cat,
     w_down,
     w_out,
     choice,
+    choice_t,
     swap,
     act,
     silu,
@@ -376,7 +382,11 @@
         pltpu.make_async_copy(down_proj.at[0], w_down, load.at[4]),
         pltpu.make_async_copy(out_proj, w_out, load.at[5]),
     ]
-    for copy in loads:
+    for n, (source, to) in enumerate(
+        ((q_hbm, q), (k_hbm, k), (v_hbm, v), (fd_hbm, fd), (bd_hbm, bd))
+    ):
+        loads.append(pltpu.make_async_copy(source, to, load.at[6 + n]))
+    for copy in (loads[0], *loads[6:], *loads[1:6]):
         copy.start()
 
     def sems(kind, i):
@@ -392,32 +402,34 @@
 
     tokens = own.shape[0]
     slots = x.shape[0]
-    lanes = iota((tokens, 128), 1)
-    first = (routes[:, 0:1] == lanes).astype(BF16)
-    second = (routes[:, 1:2] == lanes).astype(BF16)
+    names = iota((128, tokens), 0)
+    members = [(routes[j : j + 1, :] == names).astype(F32) for j in range(2)]
     shape = (tokens, tokens)
-    earlier = (iota(shape, 0) > iota(shape, 1)).astype(BF16)
-    before = dot(earlier, first + second)
-    loads[0].wait()
-    mine = own[...].astype(F32)
-    weighted = []
-    for j, members in enumerate((first, second)):
-        named = members.astype(F32)
-        rank = jnp.sum((before + first.astype(F32) * j) * named, axis=1, keepdims=True)
+    later = (iota(shape, 0) < iota(shape, 1)).astype(BF16)
+    before = dot(members[0] + members[1], later)
+    scale = jnp.zeros((slots, 1), F32)
+    chosen = jnp.zeros((slots, tokens), F32)
+    for j in range(2):
+        rank = jnp.sum((before + members[0] * j) * members[j], axis=0, keepdims=True)
         rank = rank.astype(jnp.int32)
-        expert = routes[:, j : j + 1]
+        expert = routes[j : j + 1, :]
         row = (expert & (PLANES - 1)) * CHUNK + (expert >> 3) * CAP + rank
         row = jnp.where(rank < CAP, row, -1)
-        taken = (row == iota((tokens, slots), 1)).astype(BF16)
-        choice[j * tokens : (j + 1) * tokens, :] = taken
-        weighted.append((mine * route_weight[:, j : j + 1]).astype(BF16))
-    picked = dot(choice[...], jnp.concatenate(weighted, axis=0), TN)
+        taken = row == iota((slots, tokens), 0)
+        chosen = jnp.where(taken, 1.0, chosen)
+        given = jnp.where(taken, route_weight[j : j + 1, :], 0.0)
+        scale = scale + jnp.sum(given, axis=1, keepdims=True)
+    choice[...] = chosen.astype(BF16)
+    loads[0].wait()
+    picked = dot(choice[...], own[...]) * scale
     out_plane[...] = picked.astype(BF16).reshape(out_plane.shape)
     pl.semaphore_wait(barrier, count + 2)
     for d in PLANE_ORDER:
         plane_out(0, out_plane, in_plane, d).start()
     in_plane[p] = out_plane[p]
 
+    for copy in loads[6:]:
+        copy.wait()
     pieces = [Piece(b, q, k, v, fd, bd) for b in range(3)]
     for piece in pieces:
         piece.ends()
@@ -428,6 +440,7 @@
     carry = Carry(carry_refs[:12])
     carry.start((forward_end, backward_end), (log_f, log_b))
     swap[...] = swap_matrix(swap.shape)
+    choice_t[...] = choice[...].T
 
     def chunk_of(i):
         return lax.rem(z + OFFSETS[i], DEPTH)
@@ -588,8 +601,7 @@
         up_grad_ref[rows, :] = both_grads[:, hidden:].astype(BF16)
     for d in PLANE_ORDER:
         plane_in(9, back_out, back_in, d).wait_recv()
-    taken = choice[:tokens, :] + choice[tokens:, :]
-    moe_grad = dot(taken, back_in[...].reshape(DEPTH * CHUNK, quarter))
+    moe_grad = dot(choice_t[...], back_in[...].reshape(DEPTH * CHUNK, quarter))
     stream[t] = (own[...].astype(F32) + moe_grad).astype(BF16)
 
     low, high = pl.ds(0, tokens // 2), pl.ds(tokens // 2, tokens // 2)
@@ -632,10 +644,11 @@
         return jnp.dot(stream[which], w_out[rows, :], preferred_element_type=F32)
 
     mixed_grad = share(t)
+    onward = stream_pass(left, right)
     for n, copy in enumerate(stream_arrived()):
         copy.wait_recv()
         if n < 2:
-            stream_pass(left, right)[n].start()
+            onward[n].start()
     mixed_grad = mixed_grad + share(left) + share(right)
     for copy in stream_pass(across, across):
         copy.wait_recv()
@@ -770,23 +783,25 @@
     return pl.pallas_call(
         layer_kernel,
         out_shape=(
-            jax.ShapeDtypeStruct((width, hidden), BF16),
-            jax.ShapeDtypeStruct((width, hidden), BF16),
-            jax.ShapeDtypeStruct((hidden, width), BF16),
-            jax.ShapeDtypeStruct((piece_rows, out_columns), F32),
-            jax.ShapeDtypeStruct((tokens, 128), BF16),
-            jax.ShapeDtypeStruct((tokens, 128), BF16),
-            jax.ShapeDtypeStruct((tokens, 2 * DV), BF16),
+            pltpu.VMEM((width, hidden), BF16),
+            pltpu.VMEM((width, hidden), BF16),
+            pltpu.VMEM((hidden, width), BF16),
+            pltpu.VMEM((piece_rows, out_columns), F32),
+            pltpu.VMEM((tokens, 128), BF16),
+            pltpu.VMEM((tokens, 128), BF16),
+            pltpu.VMEM((tokens, 2 * DV), BF16),
         ),
-        in_specs=vmem(2) + [anywhere] * 6 + vmem(5),
+        in_specs=vmem(2) + [anywhere] * 11,
         out_specs=tuple(vmem(7)),
         scratch_shapes=[
+            *[pltpu.VMEM(a.shape, a.dtype) for a in arrays[8:]],
             pltpu.VMEM((tokens, quarter), BF16),
             pltpu.VMEM((slots, width), BF16),
             pltpu.VMEM((width, 2 * hidden), BF16),
             pltpu.VMEM((hidden, width), BF16),
             pltpu.VMEM((width, out_columns), BF16),
-            pltpu.VMEM((2 * tokens, slots), BF16),
+            pltpu.VMEM((slots, tokens), BF16),
+            pltpu.VMEM((tokens, slots), BF16),
             pltpu.VMEM((slots, slots), BF16),
             pltpu.VMEM((DEPTH, CHUNK, hidden), BF16),
             pltpu.VMEM((DEPTH, CHUNK, hidden), F32),
@@ -807,12 +822,12 @@
             pltpu.VMEM((DEPTH, piece_rows, out_columns), F32),
             pltpu.SemaphoreType.DMA((14, DEPTH)),
             pltpu.SemaphoreType.DMA((14, DEPTH)),
-            pltpu.SemaphoreType.DMA((6,)),
+            pltpu.SemaphoreType.DMA((11,)),
             *Carry.scratch(),
             *Carry.scratch(),
         ],
         compiler_params=pltpu.CompilerParams(
-            collective_id=0, has_side_effects=True, vmem_limit_bytes=60 * 2**20
+            collective_id=0, has_side_effects=True, vmem_limit_bytes=56 * 2**20
         ),
         cost_estimate=pl.CostEstimate(
             flops=8 * 10**9, bytes_accessed=12 * 2**20, transcendentals=0
@@ -821,8 +836,33 @@
     )(*arrays)
 
 
+def write_kernel(*refs):
+    n = len(refs) // 2
+    done = refs[-1]
+    copies = [pltpu.make_async_copy(refs[i], refs[n + i], done.at[i]) for i in range(n)]
+    for copy in copies:
+        copy.start()
+    for copy in copies:
+        copy.wait()
+
+
+def written(arrays):
+    n = len(arrays)
+    arrays = [pltpu.with_memory_space_constraint(a, pltpu.VMEM) for a in arrays]
+    return pl.pallas_call(
+        write_kernel,
+        out_shape=tuple(jax.ShapeDtypeStruct(a.shape, a.dtype) for a in arrays),
+        in_specs=vmem(n),
+        out_specs=(pl.BlockSpec(memory_space=pl.ANY),) * n,
+        scratch_shapes=[pltpu.SemaphoreType.DMA((n,))],
+        compiler_params=pltpu.CompilerParams(vmem_limit_bytes=2**20),
+        name="write",
+    )(*arrays)
+
+
 def on_device(layer_grad, routes, route_weight, *arrays):
-    gate, up, down, proj, query, key, value = layer(routes, route_weight, layer_grad, *arrays)
+    results = written(layer(routes.T, route_weight.T, layer_grad, *arrays))
+    gate, up, down, proj, query, key, value = results
     return gate[None], up[None], down[None], proj, query, key, value
 
 

time: 130 us -> 120 us (0.923)
  local copies, waits for them, and re-layouts: 9.76 us -> 0 us
    unnamed x21 -> x0, local copies, waits for them, and re-layouts: 9.76 us -> none
    pallas_call x1 -> x2, Pallas kernels: 120 us -> 119 us  [the longest x1 117 us: layer(): pl.pallas_call(layer_kernel, out_shape=(pltpu.VMEM((width, hidden), BF16)...]
where the time goes in v4:
time: 120 us
  Pallas kernels  119 us (99%)
    pallas_call x1, Pallas kernels, layer(): pl.pallas_call(layer_kernel, out_shape=(pltpu.VMEM((width, hidden), BF16)...  117 us

profile of v4, /device:TPU:1, one launch (start us, length us, event | category | flops | bytes accessed | tf_op | source)
XLA Modules:
  0.0 120.0 jit_solution(14234655876600061118)
XLA Ops:
  0.6 117.4 %layer.1 = (bf16[2048,256]{1,0:T(8,128)(2,1)S(1)}, bf16[2048,256]{1,0:T(8,128)(2,1)S(1)}, bf16[256,2048]{1,0:T(8,128)(2,1)S(1)}, f32[32,256]{1,0:T(8,128)S(1)}, ...) custom-call(s32[2,192]{1,0:T(2,128)} %bitcast.8, f32[2,192]{1,0:T(2,128)} %bitcast.9, ...), custom_call_target="tpu_custom_call" | custom-call | flops 8000000000 | bytes 12582912 | tf_op jit(solution)/shard_map/layer/pallas_call | solution.py:783
  118.1 1.8 %write.1 = (bf16[2048,256]{1,0:T(8,128)(2,1)}, bf16[2048,256]{1,0:T(8,128)(2,1)}, bf16[256,2048]{1,0:T(8,128)(2,1)}, f32[32,256]{1,0:T(8,128)}, bf16[192,128]{1,...) custom-call(bf16[2048,256]{1,0:T(8,128)(2,1)S(1)} %get-tuple-element.21.refs_0_, ...), custom_call_target="tpu_custom_call" | custom-call | tf_op jit(solution)/shard_map/write/pallas_call | solution.py:852

commit v5 on v4

--- a/solution.py
+++ b/solution.py
@@ -330,7 +330,8 @@
     own,
     x,
     w_cat,
-    w_down,
+    down_out,
+    down_in,
     w_out,
     choice,
     choice_t,
@@ -343,6 +344,11 @@
     in_plane,
     out_depth,
     inbound,
+    first_part,
+    first_hop,
+    first_hopped,
+    first_both,
+    first_plain,
     part,
     hop,
     hopped,
@@ -369,24 +375,32 @@
     right, left, across = lax.rem(t + 1, RING), lax.rem(t + 3, RING), lax.rem(t + 2, RING)
     quarter = own.shape[1]
     barrier, count = greet(PLANES, DEPTH)
-    for other in (left, right):
+    for other in (left, right, across):
         pl.semaphore_signal(barrier, 1, device_id={"tp": other}, device_id_type=MESH)
 
     columns = pl.ds(pl.multiple_of(t * quarter, quarter), quarter)
-    hidden = w_down.shape[0]
+    hidden = down_in.shape[1]
     loads = [
         pltpu.make_async_copy(layer_grad.at[:, columns], own, load.at[0]),
         pltpu.make_async_copy(slot_tokens.at[0], x, load.at[1]),
         pltpu.make_async_copy(gate_proj.at[0], w_cat.at[:, pl.ds(0, hidden)], load.at[2]),
         pltpu.make_async_copy(up_proj.at[0], w_cat.at[:, pl.ds(hidden, hidden)], load.at[3]),
-        pltpu.make_async_copy(down_proj.at[0], w_down, load.at[4]),
+        pltpu.make_async_copy(down_proj.at[0, :, columns], down_in.at[t], load.at[4]),
         pltpu.make_async_copy(out_proj, w_out, load.at[5]),
     ]
     for n, (source, to) in enumerate(
         ((q_hbm, q), (k_hbm, k), (v_hbm, v), (fd_hbm, fd), (bd_hbm, bd))
     ):
         loads.append(pltpu.make_async_copy(source, to, load.at[6 + n]))
-    for copy in (loads[0], *loads[6:], *loads[1:6]):
+    for n in range(1, RING):
+        other = lax.rem(t + n, RING)
+        there = pl.ds(pl.multiple_of(other * quarter, quarter), quarter)
+        loads.append(
+            pltpu.make_async_copy(
+                down_proj.at[0, :, there], down_out.at[other], load.at[10 + n]
+            )
+        )
+    for copy in (loads[0], *loads[11:], *loads[6:11], *loads[1:6]):
         copy.start()
 
     def sems(kind, i):
@@ -423,12 +437,22 @@
     loads[0].wait()
     picked = dot(choice[...], own[...]) * scale
     out_plane[...] = picked.astype(BF16).reshape(out_plane.shape)
-    pl.semaphore_wait(barrier, count + 2)
+    pl.semaphore_wait(barrier, count + 3)
     for d in PLANE_ORDER:
         plane_out(0, out_plane, in_plane, d).start()
     in_plane[p] = out_plane[p]
 
-    for copy in loads[6:]:
+    def down_copy(n, arriving=False):
+        other = lax.rem(t + (RING - n if arriving else n), RING)
+        at = other if arriving else t
+        return remote(down_out.at[other], down_in.at[at], sems(14, n), {"tp": other})
+
+    for copy in loads[11:]:
+        copy.wait()
+    for n in (2, 1, 3):
+        down_copy(n).start()
+
+    for copy in loads[6:11]:
         copy.wait()
     pieces = [Piece(b, q, k, v, fd, bd) for b in range(3)]
     for piece in pieces:
@@ -478,24 +502,41 @@
         other = chunk_of(i)
         return remote(ret_out.at[other], ret_in.at[at], sems(8, i), {"sp_0": other})
 
+    def first_send_hop(i):
+        _, to = sides(i)
+        return remote(first_part.at[i, across], first_hop.at[i], sems(15, i), {"tp": to})
+
+    def first_send_both(i):
+        _, to = sides(i)
+        return remote(first_hopped.at[i], first_both.at[i], sems(16, i), {"tp": to})
+
+    def first_send_plain(i):
+        to, _ = sides(i)
+        return remote(first_part.at[i, to], first_plain.at[i], sems(17, i), {"tp": to})
+
     def stage_0(i):
+        at = chunk_of(i)
         if i > 0:
-            at = chunk_of(i)
             remote(out_depth.at[at], inbound.at[t, at], sems(1, i), {"sp_0": at}).wait_recv()
-        for copy in spread(i):
-            copy.start()
+        partial = dot(inbound[t, at], down_in[...].reshape(RING * hidden, quarter), NT)
+        for n in range(RING):
+            first_part[i, n] = partial[:, n * hidden : (n + 1) * hidden].astype(BF16)
+        first_send_hop(i).start()
+        first_send_plain(i).start()
 
     def stage_1(i):
-        for copy in spread(i, True):
-            copy.wait_recv()
-        pass_on(i).start()
+        _, to = sides(i)
+        first_send_hop(i).wait_recv()
+        total = first_hop[i].astype(F32) + first_part[i, to].astype(F32)
+        first_hopped[i] = total.astype(BF16)
+        first_send_both(i).start()
 
     def stage_2(i):
         at = chunk_of(i)
-        pass_on(i, True).wait_recv()
-        total = jnp.zeros((CHUNK, hidden), F32)
-        for n in range(RING):
-            total = total + dot(inbound[n, at], w_down[:, n * quarter : (n + 1) * quarter], NT)
+        first_send_both(i).wait_recv()
+        first_send_plain(i).wait_recv()
+        total = first_part[i, t].astype(F32) + first_both[i].astype(F32)
+        total = total + first_plain[i].astype(F32)
         up_delta = (total * silu[at]).astype(BF16)
         gate_delta = (total * slope[at]).astype(BF16)
         deltas = jnp.concatenate([gate_delta, up_delta], axis=1)
@@ -536,7 +577,6 @@
         return remote(out_depth.at[other], inbound.at[t, z], sems(1, i), {"sp_0": other})
 
     inbound[t, z] = out_depth[z]
-    stage_0(0)
     for i in range(1, DEPTH):
         depth_out(i).start()
     carry.middle()
@@ -556,11 +596,13 @@
         act[chunks] = (s * up).astype(BF16).reshape(shape)
         slope[chunks] = (up * sigma * (1.0 + gate * (1.0 - sigma))).reshape(shape)
     loads[4].wait()
+    for n in range(1, RING):
+        down_copy(n, True).wait_recv()
 
     stages = (stage_0, stage_1, stage_2, stage_3, stage_4)
     for n in range(DEPTH + len(stages) - 1):
         for lag, stage in enumerate(stages):
-            if 0 <= n - lag < DEPTH and (n > 0 or lag > 0):
+            if 0 <= n - lag < DEPTH:
                 stage(n - lag)
         if n == 2:
             inclusive, strict = masks()
@@ -581,10 +623,9 @@
                 piece.inv = lax.rsqrt(jnp.mean(o * o, axis=1, keepdims=True) + EPSILON)
                 piece.mixed = o * piece.inv
 
-    act_all = act[...].reshape(DEPTH * CHUNK, hidden)
-    for n in range(RING):
-        rows = inbound[n].reshape(DEPTH * CHUNK, quarter)
-        down_grad_ref[:, n * quarter : (n + 1) * quarter] = dot(act_all, rows, TN).astype(BF16)
+    for i in range(DEPTH):
+        for copy in spread(i):
+            copy.start()
 
     for i in range(1, DEPTH):
         send_back(i, True).wait_recv()
@@ -693,6 +734,10 @@
         return remote(row_sum.at[other], depth_in.at[at], sems(13, d), {"sp_0": other})
 
     core_copy().start()
+    for i in range(DEPTH):
+        for copy in spread(i, True):
+            copy.wait_recv()
+        pass_on(i).start()
 
     inclusive, strict = masks()
     for piece in pieces:
@@ -716,13 +761,19 @@
         dq = piece.dq + dq[:, :128] * stacked(piece.eg) + dq[:, 128:] * stacked(piece.eh)
         dq_ref[pl.ds(b * BLOCK, BLOCK), :] = (folded(dq) * KEY_CHANNELS**-0.5).astype(BF16)
     carry.last()
+    for i in range(DEPTH):
+        pass_on(i, True).wait_recv()
+    act_all = act[...].reshape(DEPTH * CHUNK, hidden)
+    for n in range(RING):
+        rows = inbound[n].reshape(DEPTH * CHUNK, quarter)
+        down_grad_ref[:, n * quarter : (n + 1) * quarter] = dot(act_all, rows, TN).astype(BF16)
     for d in (1, 3, 2):
         row_copy(d, True).wait_recv()
     row_in[y] = core_sum[y]
     total = row_in[0].astype(F32)
     for n in range(1, 4):
         total = total + row_in[n].astype(F32)
-    row_sum[...] = total
+    row_sum[...] = total.astype(BF16)
     for d in (4, 3, 5, 2, 6, 1, 7):
         last_copy(d).start()
     back_c, back_d = carry.finish()
@@ -744,9 +795,9 @@
     depth_in[z] = row_sum[z]
     for d in range(1, DEPTH):
         last_copy(d, True).wait_recv()
-    total = depth_in[0]
+    total = depth_in[0].astype(F32)
     for n in range(1, DEPTH):
-        total = total + depth_in[n]
+        total = total + depth_in[n].astype(F32)
     proj_ref[...] = total
 
     for d in PLANE_ORDER:
@@ -758,6 +809,10 @@
             send_back(i).wait_send()
         for copy in (*spread(i), pass_on(i), send_hop(i), send_both(i), send_plain(i)):
             copy.wait_send()
+        for copy in (first_send_hop(i), first_send_both(i), first_send_plain(i)):
+            copy.wait_send()
+    for n in range(1, RING):
+        down_copy(n).wait_send()
     for copy in (*stream_spread(), *stream_pass(left, right), core_copy()):
         copy.wait_send()
     for d in (1, 2, 3):
@@ -798,7 +853,8 @@
             pltpu.VMEM((tokens, quarter), BF16),
             pltpu.VMEM((slots, width), BF16),
             pltpu.VMEM((width, 2 * hidden), BF16),
-            pltpu.VMEM((hidden, width), BF16),
+            pltpu.VMEM((RING, hidden, quarter), BF16),
+            pltpu.VMEM((RING, hidden, quarter), BF16),
             pltpu.VMEM((width, out_columns), BF16),
             pltpu.VMEM((slots, tokens), BF16),
             pltpu.VMEM((tokens, slots), BF16),
@@ -811,6 +867,8 @@
             pltpu.VMEM(rows, BF16),
             pltpu.VMEM(rows, BF16),
             pltpu.VMEM((RING, *rows), BF16),
+            pltpu.VMEM((DEPTH, RING, CHUNK, hidden), BF16),
+            *[pltpu.VMEM((DEPTH, CHUNK, hidden), BF16)] * 4,
             pltpu.VMEM((DEPTH, RING, CHUNK, quarter), BF16),
             *[pltpu.VMEM(rows, BF16)] * 8,
             pltpu.VMEM((RING, tokens, quarter), BF16),
@@ -818,11 +876,11 @@
             pltpu.VMEM((4, DEPTH, piece_rows, out_columns), BF16),
             pltpu.VMEM((4, DEPTH, piece_rows, out_columns), BF16),
             pltpu.VMEM((4, DEPTH, piece_rows, out_columns), BF16),
-            pltpu.VMEM((DEPTH, piece_rows, out_columns), F32),
-            pltpu.VMEM((DEPTH, piece_rows, out_columns), F32),
-            pltpu.SemaphoreType.DMA((14, DEPTH)),
-            pltpu.SemaphoreType.DMA((14, DEPTH)),
-            pltpu.SemaphoreType.DMA((11,)),
+            pltpu.VMEM((DEPTH, piece_rows, out_columns), BF16),
+            pltpu.VMEM((DEPTH, piece_rows, out_columns), BF16),
+            pltpu.SemaphoreType.DMA((18, DEPTH)),
+            pltpu.SemaphoreType.DMA((18, DEPTH)),
+            pltpu.SemaphoreType.DMA((14,)),
             *Carry.scratch(),
             *Carry.scratch(),
         ],

time: 120 us -> 111 us (0.925)
  Pallas kernels: 119 us -> 110 us
    pallas_call x1, Pallas kernels: 117 us -> 108 us  [layer(): pl.pallas_call(layer_kernel, out_shape=(pltpu.VMEM((width, hidden), BF16)...]
where the time goes in v5:
time: 111 us
  Pallas kernels  110 us (99%)
    pallas_call x1, Pallas kernels, layer(): pl.pallas_call(layer_kernel, out_shape=(pltpu.VMEM((width, hidden), BF16)...  108 us

profile of v5, /device:TPU:1, one launch (start us, length us, event | category | flops | bytes accessed | tf_op | source)
XLA Modules:
  0.0 111.0 jit_solution(9926242275307597053)
XLA Ops:
  0.6 108.4 %layer.1 = (bf16[2048,256]{1,0:T(8,128)(2,1)S(1)}, bf16[2048,256]{1,0:T(8,128)(2,1)S(1)}, bf16[256,2048]{1,0:T(8,128)(2,1)S(1)}, f32[32,256]{1,0:T(8,128)S(1)}, ...) custom-call(s32[2,192]{1,0:T(2,128)} %bitcast.8, f32[2,192]{1,0:T(2,128)} %bitcast.9, ...), custom_call_target="tpu_custom_call" | custom-call | flops 8000000000 | bytes 12582912 | tf_op jit(solution)/shard_map/layer/pallas_call | solution.py:838
  109.0 1.8 %write.1 = (bf16[2048,256]{1,0:T(8,128)(2,1)}, bf16[2048,256]{1,0:T(8,128)(2,1)}, bf16[256,2048]{1,0:T(8,128)(2,1)}, f32[32,256]{1,0:T(8,128)}, bf16[192,128]{1,...) custom-call(bf16[2048,256]{1,0:T(8,128)(2,1)S(1)} %get-tuple-element.21.refs_0_, ...), custom_call_target="tpu_custom_call" | custom-call | tf_op jit(solution)/shard_map/write/pallas_call | solution.py:910

commit v6 on v5

--- a/solution.py
+++ b/solution.py
@@ -274,7 +274,15 @@
         return [self.in3[:, dim].reshape(128, 128) for dim in range(2)]
 
 
-OFFSETS = (0, 1, 7, 2, 6, 3, 5, 4)
+OFFSETS = (0, 7, 3, 4, 5, 2, 6, 1)
+AWAY = tuple(i for i, offset in enumerate(OFFSETS) if offset)
+OWN = OFFSETS.index(0)
+SCHEDULE = (
+    ((0, 0), (0, 1), (1, 0), (1, 1), (0, 2), (2, 0), (2, 1), (0, 3), (0, 4), (1, 2), (0, 8))
+    + ((0, 7), (0, 6), (1, 3), (0, 5), (1, 4), (2, 2), (1, 6), (2, 3), (1, 5), (3, 1), (2, 4))
+    + ((3, 2), (3, 3), (1, 7), (2, 5), (1, 8), (4, 1), (3, 4), (2, 6), (4, 2), (2, 8), (4, 3))
+    + ((2, 7), (4, 4), (3, 5), (3, 6), (3, 0), (3, 7), (4, 5), (4, 6), (4, 0), (4, 7))
+)
 PLANE_ORDER = (2, 6, 3, 7, 4, 5, 1)
 PLANES, DEPTH, RING = 8, 8, 4
 CHUNK = PLANES * CAP
@@ -516,7 +524,7 @@
 
     def stage_0(i):
         at = chunk_of(i)
-        if i > 0:
+        if i != OWN:
             remote(out_depth.at[at], inbound.at[t, at], sems(1, i), {"sp_0": at}).wait_recv()
         partial = dot(inbound[t, at], down_in[...].reshape(RING * hidden, quarter), NT)
         for n in range(RING):
@@ -561,7 +569,7 @@
         send_both(i).wait_recv()
         send_plain(i).wait_recv()
         total = part[i, t].astype(F32) + both[i].astype(F32) + plain[i].astype(F32)
-        if i == 0:
+        if i == OWN:
             ret_in[z] = total.astype(BF16)
         else:
             ret_out[at] = total.astype(BF16)
@@ -577,9 +585,8 @@
         return remote(out_depth.at[other], inbound.at[t, z], sems(1, i), {"sp_0": other})
 
     inbound[t, z] = out_depth[z]
-    for i in range(1, DEPTH):
+    for i in AWAY:
         depth_out(i).start()
-    carry.middle()
 
     for copy in loads[1:4]:
         copy.wait()
@@ -599,35 +606,38 @@
     for n in range(1, RING):
         down_copy(n, True).wait_recv()
 
-    stages = (stage_0, stage_1, stage_2, stage_3, stage_4)
-    for n in range(DEPTH + len(stages) - 1):
-        for lag, stage in enumerate(stages):
-            if 0 <= n - lag < DEPTH:
-                stage(n - lag)
-        if n == 2:
+    def attend(step):
+        if step == 0:
+            carry.middle()
+        elif step == 1:
             inclusive, strict = masks()
             for piece in pieces:
                 piece.a = piece.scores(inclusive, strict)
                 piece.inner = dot(piece.a, piece.vs)
                 piece.entries()
-        if n == 5:
+        else:
             carry.last()
-        if n == 8:
-            forward_entry, backward_entry = carry.finish()
-            before, after, _, _ = both_states(pieces, forward_entry, backward_entry)
-            for b, piece in enumerate(pieces):
-                piece.states = jnp.concatenate([before[b], after[b]], axis=1).astype(BF16)
-                o = piece.inner + dot(
-                    jnp.concatenate([piece.qg, piece.qh], axis=1), piece.states, NT
-                )
-                piece.inv = lax.rsqrt(jnp.mean(o * o, axis=1, keepdims=True) + EPSILON)
-                piece.mixed = o * piece.inv
+
+    stages = (stage_0, stage_1, stage_2, stage_3, stage_4)
+    for stage, i in SCHEDULE:
+        if i == DEPTH:
+            attend(stage)
+        else:
+            stages[stage](i)
 
     for i in range(DEPTH):
         for copy in spread(i):
             copy.start()
 
-    for i in range(1, DEPTH):
+    forward_entry, backward_entry = carry.finish()
+    before, after, _, _ = both_states(pieces, forward_entry, backward_entry)
+    for b, piece in enumerate(pieces):
+        piece.states = jnp.concatenate([before[b], after[b]], axis=1).astype(BF16)
+        o = piece.inner + dot(jnp.concatenate([piece.qg, piece.qh], axis=1), piece.states, NT)
+        piece.inv = lax.rsqrt(jnp.mean(o * o, axis=1, keepdims=True) + EPSILON)
+        piece.mixed = o * piece.inv
+
+    for i in AWAY:
         send_back(i, True).wait_recv()
     moved = dot(swap[...], ret_in[...].reshape(DEPTH * CHUNK, quarter)).astype(BF16)
     back_out[...] = moved.reshape(back_out.shape)
@@ -648,22 +658,23 @@
     low, high = pl.ds(0, tokens // 2), pl.ds(tokens // 2, tokens // 2)
 
     def ring(kind, which, rows, to):
-        return remote(stream.at[which, rows], stream.at[which, rows], sems(kind, 0), {"tp": to})
+        pair = sems(kind, 0 if kind in (0, 9) else OWN)
+        return remote(stream.at[which, rows], stream.at[which, rows], pair, {"tp": to})
 
     def stream_spread():
         return (
             ring(0, t, low, right),
             ring(1, t, high, left),
-            ring(2 + 6, t, high, right),
-            ring(3 + 6, t, low, left),
+            ring(8, t, high, right),
+            ring(9, t, low, left),
         )
 
     def stream_arrived():
         return (
             ring(0, left, low, right),
             ring(1, right, high, left),
-            ring(2 + 6, left, high, right),
-            ring(3 + 6, right, low, left),
+            ring(8, left, high, right),
+            ring(9, right, low, left),
         )
 
     def stream_pass(which_low, which_high):
@@ -734,6 +745,10 @@
         return remote(row_sum.at[other], depth_in.at[at], sems(13, d), {"sp_0": other})
 
     core_copy().start()
+    core_copy().wait_recv()
+    core_sum[...] = (terms[c].astype(F32) + core_in[...].astype(F32)).astype(BF16)
+    for d in (2, 1, 3):
+        row_copy(d).start()
     for i in range(DEPTH):
         for copy in spread(i, True):
             copy.wait_recv()
@@ -752,21 +767,11 @@
             da_b, piece.q_up_h, TN
         ) * doubled(piece.dn_h)
     carry.middle()
-    core_copy().wait_recv()
-    core_sum[...] = (terms[c].astype(F32) + core_in[...].astype(F32)).astype(BF16)
-    for d in (2, 1, 3):
-        row_copy(d).start()
     for b, piece in enumerate(pieces):
         dq = dot(piece.do, piece.states)
         dq = piece.dq + dq[:, :128] * stacked(piece.eg) + dq[:, 128:] * stacked(piece.eh)
         dq_ref[pl.ds(b * BLOCK, BLOCK), :] = (folded(dq) * KEY_CHANNELS**-0.5).astype(BF16)
     carry.last()
-    for i in range(DEPTH):
-        pass_on(i, True).wait_recv()
-    act_all = act[...].reshape(DEPTH * CHUNK, hidden)
-    for n in range(RING):
-        rows = inbound[n].reshape(DEPTH * CHUNK, quarter)
-        down_grad_ref[:, n * quarter : (n + 1) * quarter] = dot(act_all, rows, TN).astype(BF16)
     for d in (1, 3, 2):
         row_copy(d, True).wait_recv()
     row_in[y] = core_sum[y]
@@ -776,6 +781,12 @@
     row_sum[...] = total.astype(BF16)
     for d in (4, 3, 5, 2, 6, 1, 7):
         last_copy(d).start()
+    for i in range(DEPTH):
+        pass_on(i, True).wait_recv()
+    act_all = act[...].reshape(DEPTH * CHUNK, hidden)
+    for n in range(RING):
+        rows = inbound[n].reshape(DEPTH * CHUNK, quarter)
+        down_grad_ref[:, n * quarter : (n + 1) * quarter] = dot(act_all, rows, TN).astype(BF16)
     back_c, back_d = carry.finish()
     late, early = [None] * 3, [None] * 3
     for b, piece in enumerate(pieces):
@@ -804,7 +815,7 @@
         plane_out(0, out_plane, in_plane, d).wait_send()
         plane_out(9, back_out, back_in, d).wait_send()
     for i in range(DEPTH):
-        if i > 0:
+        if i != OWN:
             depth_out(i).wait_send()
             send_back(i).wait_send()
         for copy in (*spread(i), pass_on(i), send_hop(i), send_both(i), send_plain(i)):

time: 111 us -> 106 us (0.955)
  Pallas kernels: 110 us -> 105 us
    pallas_call x1, Pallas kernels: 108 us -> 103 us  [layer(): pl.pallas_call(layer_kernel, out_shape=(pltpu.VMEM((width, hidden), BF16)...]
where the time goes in v6:
time: 106 us
  Pallas kernels  105 us (99%)
    pallas_call x1, Pallas kernels, layer(): pl.pallas_call(layer_kernel, out_shape=(pltpu.VMEM((width, hidden), BF16)...  103 us

profile of v6, /device:TPU:1, one launch (start us, length us, event | category | flops | bytes accessed | tf_op | source)
XLA Modules:
  0.0 105.9 jit_solution(11260712842760292521)
XLA Ops:
  0.6 103.3 %layer.1 = (bf16[2048,256]{1,0:T(8,128)(2,1)S(1)}, bf16[2048,256]{1,0:T(8,128)(2,1)S(1)}, bf16[256,2048]{1,0:T(8,128)(2,1)S(1)}, f32[32,256]{1,0:T(8,128)S(1)}, ...) custom-call(s32[2,192]{1,0:T(2,128)} %bitcast.8, f32[2,192]{1,0:T(2,128)} %bitcast.9, ...), custom_call_target="tpu_custom_call" | custom-call | flops 8000000000 | bytes 12582912 | tf_op jit(solution)/shard_map/layer/pallas_call | solution.py:849
  104.0 1.8 %write.1 = (bf16[2048,256]{1,0:T(8,128)(2,1)}, bf16[2048,256]{1,0:T(8,128)(2,1)}, bf16[256,2048]{1,0:T(8,128)(2,1)}, f32[32,256]{1,0:T(8,128)}, bf16[192,128]{1,...) custom-call(bf16[2048,256]{1,0:T(8,128)(2,1)S(1)} %get-tuple-element.21.refs_0_, ...), custom_call_target="tpu_custom_call" | custom-call | tf_op jit(solution)/shard_map/write/pallas_call | solution.py:921

commit v7 on v6

--- a/solution.py
+++ b/solution.py
@@ -208,7 +208,7 @@
             for j in range(self.n):
                 self.out1[j, dim, :PIECE, :] = terms[dim][j * PIECE : (j + 1) * PIECE, :]
                 self.out1[j, dim, PIECE:, :] = decay
-        for d in range(1, self.n):
+        for d in PLANE_ORDER:
             self.plane_copy(self.out1, self.in1, self.s1, self.r1, d).start()
         self.in1[self.p] = self.out1[self.p]
 
@@ -227,7 +227,7 @@
                 log = log + step
             self.out2[dim, :PIECE, :] = total
             self.out2[dim, PIECE:, :] = jnp.broadcast_to(log, (8, 128))
-        for d in range(1, self.m):
+        for d in DEPTH_ORDER:
             self.depth_copy(d).start()
 
     def depth_copy(self, d, arriving=False):
@@ -259,7 +259,7 @@
             for dim in range(2):
                 inside, log = self.before[dim][i]
                 self.out3[i, dim] = inside + jnp.exp(log) * entry[dim]
-        for d in range(1, self.n):
+        for d in PLANE_ORDER:
             self.plane_copy(self.out3, self.in3, self.s3, self.r3, d).start()
         self.in3[self.p] = self.out3[self.p]
 
@@ -283,7 +283,8 @@
     + ((3, 2), (3, 3), (1, 7), (2, 5), (1, 8), (4, 1), (3, 4), (2, 6), (4, 2), (2, 8), (4, 3))
     + ((2, 7), (4, 4), (3, 5), (3, 6), (3, 0), (3, 7), (4, 5), (4, 6), (4, 0), (4, 7))
 )
-PLANE_ORDER = (2, 6, 3, 7, 4, 5, 1)
+PLANE_ORDER = (4, 5, 2, 6, 3, 7, 1)
+DEPTH_ORDER = (4, 3, 5, 2, 6, 1, 7)
 PLANES, DEPTH, RING = 8, 8, 4
 CHUNK = PLANES * CAP
 MESH = pl.DeviceIdType.MESH
@@ -687,8 +688,43 @@
             ),
         )
 
+    rows_of_mixed = jnp.concatenate([heads_on_lanes(piece.mixed) for piece in pieces], axis=0)
+    rows_of_mixed = rows_of_mixed.astype(BF16)
+    piece_rows = proj_ref.shape[0]
+    per = quarter // (piece_rows * PLANES)
+    turns = (t, left, right, across)
+
+    def span(n):
+        return pl.ds(turns[n] * per, per)
+
+    def make_terms(n):
+        term = dot(stream[turns[n]], rows_of_mixed, TN).astype(BF16)
+        term = term.reshape(per, 4, 2, piece_rows, term.shape[1])
+        for cc in range(2):
+            for zz in range(per):
+                terms[cc, :, turns[n] * per + zz] = term[zz, :, cc]
+        core_copy(n).start()
+
+    def core_copy(n):
+        src, dst = terms.at[1 - c, :, span(n)], core_in.at[:, span(n)]
+        return remote(src, dst, sems(12, n), {"sp_2": 1 - c})
+
+    def row_copy(n, d, arriving=False):
+        other = lax.rem(y + (4 - d if arriving else d), 4)
+        at = other if arriving else y
+        src, dst = core_sum.at[other, span(n)], row_in.at[at, span(n)]
+        return remote(src, dst, sems(18 + n, d), {"sp_1": other})
+
+    def send_terms(n):
+        core_copy(n).wait_recv()
+        mine = terms[c, :, span(n)].astype(F32)
+        core_sum[:, span(n)] = (mine + core_in[:, span(n)].astype(F32)).astype(BF16)
+        for d in (2, 1, 3):
+            row_copy(n, d).start()
+
     for copy in stream_spread():
         copy.start()
+    make_terms(0)
     loads[5].wait()
 
     def share(which):
@@ -701,7 +737,10 @@
         copy.wait_recv()
         if n < 2:
             onward[n].start()
+    make_terms(1)
+    make_terms(2)
     mixed_grad = mixed_grad + share(left) + share(right)
+    send_terms(0)
     for copy in stream_pass(across, across):
         copy.wait_recv()
     mixed_grad = mixed_grad + share(across)
@@ -719,40 +758,14 @@
         back_d = back_d * jnp.exp(piece.last) + piece.back_f
     carry = Carry(carry_refs[12:])
     carry.start((back_c, back_d), (log_b, log_f))
-
-    rows_of_mixed = jnp.concatenate([heads_on_lanes(piece.mixed) for piece in pieces], axis=0)
-    rows_of_mixed = rows_of_mixed.astype(BF16)
-    piece_rows = proj_ref.shape[0]
-    for n in range(RING):
-        term = dot(stream[n], rows_of_mixed, TN).astype(BF16)
-        per = term.shape[0] // (piece_rows * PLANES)
-        term = term.reshape(per, 4, 2, piece_rows, term.shape[1])
-        for cc in range(2):
-            for zz in range(per):
-                terms[cc, :, n * per + zz] = term[zz, :, cc]
-
-    def core_copy():
-        return remote(terms.at[1 - c], core_in, sems(12, 0), {"sp_2": 1 - c})
-
-    def row_copy(d, arriving=False):
-        other = lax.rem(y + (4 - d if arriving else d), 4)
-        at = other if arriving else y
-        return remote(core_sum.at[other], row_in.at[at], sems(12, d), {"sp_1": other})
+    make_terms(3)
+    send_terms(1)
+    send_terms(2)
 
     def last_copy(d, arriving=False):
         other = lax.rem(z + (DEPTH - d if arriving else d), DEPTH)
         at = other if arriving else z
         return remote(row_sum.at[other], depth_in.at[at], sems(13, d), {"sp_0": other})
-
-    core_copy().start()
-    core_copy().wait_recv()
-    core_sum[...] = (terms[c].astype(F32) + core_in[...].astype(F32)).astype(BF16)
-    for d in (2, 1, 3):
-        row_copy(d).start()
-    for i in range(DEPTH):
-        for copy in spread(i, True):
-            copy.wait_recv()
-        pass_on(i).start()
 
     inclusive, strict = masks()
     for piece in pieces:
@@ -766,21 +779,28 @@
         piece.dk = dot(da_f, piece.q_up_g, TN) * doubled(piece.dn_g) + dot(
             da_b, piece.q_up_h, TN
         ) * doubled(piece.dn_h)
+    send_terms(3)
+    for i in range(DEPTH):
+        for copy in spread(i, True):
+            copy.wait_recv()
+        pass_on(i).start()
+
     carry.middle()
     for b, piece in enumerate(pieces):
         dq = dot(piece.do, piece.states)
         dq = piece.dq + dq[:, :128] * stacked(piece.eg) + dq[:, 128:] * stacked(piece.eh)
         dq_ref[pl.ds(b * BLOCK, BLOCK), :] = (folded(dq) * KEY_CHANNELS**-0.5).astype(BF16)
-    carry.last()
-    for d in (1, 3, 2):
-        row_copy(d, True).wait_recv()
+    for n in range(4):
+        for d in (1, 3, 2):
+            row_copy(n, d, True).wait_recv()
     row_in[y] = core_sum[y]
     total = row_in[0].astype(F32)
     for n in range(1, 4):
         total = total + row_in[n].astype(F32)
     row_sum[...] = total.astype(BF16)
-    for d in (4, 3, 5, 2, 6, 1, 7):
+    for d in DEPTH_ORDER:
         last_copy(d).start()
+    carry.last()
     for i in range(DEPTH):
         pass_on(i, True).wait_recv()
     act_all = act[...].reshape(DEPTH * CHUNK, hidden)
@@ -824,10 +844,12 @@
             copy.wait_send()
     for n in range(1, RING):
         down_copy(n).wait_send()
-    for copy in (*stream_spread(), *stream_pass(left, right), core_copy()):
+    for copy in (*stream_spread(), *stream_pass(left, right)):
         copy.wait_send()
-    for d in (1, 2, 3):
-        row_copy(d).wait_send()
+    for n in range(4):
+        core_copy(n).wait_send()
+        for d in (1, 2, 3):
+            row_copy(n, d).wait_send()
     for d in range(1, DEPTH):
         last_copy(d).wait_send()
 
@@ -889,8 +911,8 @@
             pltpu.VMEM((4, DEPTH, piece_rows, out_columns), BF16),
             pltpu.VMEM((DEPTH, piece_rows, out_columns), BF16),
             pltpu.VMEM((DEPTH, piece_rows, out_columns), BF16),
-            pltpu.SemaphoreType.DMA((18, DEPTH)),
-            pltpu.SemaphoreType.DMA((18, DEPTH)),
+            pltpu.SemaphoreType.DMA((22, DEPTH)),
+            pltpu.SemaphoreType.DMA((22, DEPTH)),
             pltpu.SemaphoreType.DMA((14,)),
             *Carry.scratch(),
             *Carry.scratch(),

time: 106 us -> 105 us (level)
  no operation moved by 1% of the time
where the time goes in v7:
time: 105 us
  Pallas kernels  104 us (99%)
    pallas_call x1, Pallas kernels, layer(): pl.pallas_call(layer_kernel, out_shape=(pltpu.VMEM((width, hidden), BF16)...  103 us

profile of v7, /device:TPU:1, one launch (start us, length us, event | category | flops | bytes accessed | tf_op | source)
XLA Modules:
  0.0 105.1 jit_solution(472350572126389387)
XLA Ops:
  0.6 102.5 %layer.1 = (bf16[2048,256]{1,0:T(8,128)(2,1)S(1)}, bf16[2048,256]{1,0:T(8,128)(2,1)S(1)}, bf16[256,2048]{1,0:T(8,128)(2,1)S(1)}, f32[32,256]{1,0:T(8,128)S(1)}, ...) custom-call(s32[2,192]{1,0:T(2,128)} %bitcast.8, f32[2,192]{1,0:T(2,128)} %bitcast.9, ...), custom_call_target="tpu_custom_call" | custom-call | flops 8000000000 | bytes 12582912 | tf_op jit(solution)/shard_map/layer/pallas_call | solution.py:871
  103.2 1.8 %write.1 = (bf16[2048,256]{1,0:T(8,128)(2,1)}, bf16[2048,256]{1,0:T(8,128)(2,1)}, bf16[256,2048]{1,0:T(8,128)(2,1)}, f32[32,256]{1,0:T(8,128)}, bf16[192,128]{1,...) custom-call(bf16[2048,256]{1,0:T(8,128)(2,1)S(1)} %get-tuple-element.21.refs_0_, ...), custom_call_target="tpu_custom_call" | custom-call | tf_op jit(solution)/shard_map/write/pallas_call | solution.py:943
